TPU v7x, 128 devices: a whole 4x4x4 slice. The times are simulated.
128 devices in a mesh: sp: 32 (over z, y, core), tp: 4 (over x).
Axes of the slice: x: 4, y: 4, z: 4, core: 2. Of those that a mesh axis runs over, the one named last changes fastest.
Arguments:
- queries: bfloat16 [16384, 1024], P('sp', 'tp'), may hold values from -260 to 260, as said below
- keys: bfloat16 [16384, 512], P('sp', 'tp'), may hold values from -8 to 8, as said below
- values: bfloat16 [16384, 512], P('sp', 'tp'), may hold values from -24 to 24
- doc_ids: int32 [16384], P('sp'), may hold values from 0 to 7, never falling along the last dimension, each value on 1 to 8192 neighbouring positions
- sink_logit: float32 [8], P('tp'), may hold values from 2 to 7
- residual_in: bfloat16 [16384, 2048], P(('sp', 'tp')), may hold values from -6 to 6
- w_out: bfloat16 [1024, 2048], replicated, may hold values from -0.375 to 0.375
- gain_one: float32 [2048], replicated, may hold values from 0.1 to 1.9
- w_gate: bfloat16 [2048, 5632], P('sp', 'tp'), may hold values from -0.125 to 0.125
- w_up: bfloat16 [2048, 5632], P('sp', 'tp'), may hold values from -0.125 to 0.125
- w_down: bfloat16 [5632, 2048], P('tp', 'sp'), may hold values from -0.078125 to 0.078125
- gain_two: float32 [2048], replicated, may hold values from 0.1 to 1.9
Outputs:
- layer_out: bfloat16 [16384, 2048], P(('sp', 'tp'))
Inputs may be any that keep to these rules, and one draw needn't show every extreme that they name: Real-valued projected queries. Real-valued projected keys. `doc_ids`: document numbers never fall along the sequence; each document is one run of positions.
All inputs are finite; a program needn't handle non-finite values.
Results may differ from a plain program's by a relative error of at most 0.012.
Values may be sent and summed in bfloat16 or wider, within the bound.
A program may use at most 128 MiB of HBM per device.

v0:
```python
import functools
import math

import jax
import jax.numpy as jnp
from jax import lax
from jax.experimental import pallas as pl
from jax.experimental.pallas import tpu as pltpu
from jax.sharding import PartitionSpec as P

HEAD = 128
HALF = 128
CORES = 2
ALPHA = 2.0**0.5
EPS = 1e-05
NEGATIVE = -1e30
MESH = pl.DeviceIdType.MESH


def layer_norm(values_in, gain):
    average = jnp.mean(values_in, -1, keepdims=True)
    centred = values_in - average
    variance = jnp.mean(centred * centred, -1, keepdims=True)
    return centred * lax.rsqrt(variance + EPS) * gain


def kernel(
    sp_size,
    tp_size,
    q_ref,
    sink_ref,
    res_ref,
    gain_one_ref,
    gain_two_ref,
    k_hbm,
    v_hbm,
    doc_row_hbm,
    w_out_hbm,
    wg_hbm,
    wu_hbm,
    wd_hbm,
    out_ref,
    k_all,
    v_all,
    doc_all,
    w_out,
    gate_w,
    up_w,
    down_w,
    att,
    tokens,
    pre,
    normed,
    hidden,
    down_in,
    parts,
    others,
    local_sem,
    halo_send,
    halo_recv,
    ring_send,
    ring_recv,
    pair_send,
    pair_recv,
    tok_send,
    tok_recv,
    norm_send,
    norm_recv,
    sum_send,
    sum_recv,
):
    sp = lax.axis_index("sp")
    tp = lax.axis_index("tp")
    chips = sp_size // CORES
    y_size = math.gcd(tp_size, chips)
    z_size = chips // y_size
    half_ring = chips // 2
    core = lax.rem(sp, CORES)
    chip = sp // CORES
    my_y = lax.rem(chip, y_size)
    my_z = chip // y_size
    odd = lax.rem(my_y, 2)
    pos = my_y * z_size + my_z * (1 - odd) + (z_size - 1 - my_z) * odd

    def chip_at(steps):
        p = lax.rem(pos + (chips + steps), chips)
        y = p // z_size
        along = lax.rem(p, z_size)
        turned = lax.rem(y, 2)
        z = along * (1 - turned) + (z_size - 1 - along) * turned
        return z * y_size + y

    rows = q_ref.shape[0]
    token_rows = res_ref.shape[0]
    depth = wg_hbm.shape[0]
    cols_tp = q_ref.shape[1]
    kv_local = k_hbm.shape[1] // HEAD
    repeat = q_ref.shape[1] // k_hbm.shape[1]
    width = res_ref.shape[1]

    forward = (chip_at(1) * CORES + core, tp)
    backward = (chip_at(-1) * CORES + core, tp)
    partner = (chip * CORES + (1 - core), tp)
    after = (lax.rem(sp + 1, sp_size), tp)
    before = (lax.rem(sp + sp_size - 1, sp_size), tp)
    peers = [lax.rem(tp + i, tp_size) for i in range(1, tp_size)]

    barrier = pltpu.get_barrier_semaphore()
    greeted = [forward, backward, partner, after, before] + [(sp, j) for j in peers]
    for device in greeted:
        pl.semaphore_signal(barrier, inc=1, device_id=device, device_id_type=MESH)

    loads = [
        pltpu.make_async_copy(k_hbm, k_all.at[pl.ds(HALF, rows)], local_sem.at[0]),
        pltpu.make_async_copy(v_hbm, v_all.at[pl.ds(HALF, rows)], local_sem.at[1]),
        pltpu.make_async_copy(doc_row_hbm, doc_all.at[:, pl.ds(HALF, rows)], local_sem.at[2]),
        pltpu.make_async_copy(w_out_hbm, w_out, local_sem.at[3]),
    ]
    mine = pl.multiple_of(sp * depth, depth)
    own_loads = [
        pltpu.make_async_copy(src, dst.at[pl.ds(mine, depth)], local_sem.at[4 + i])
        for i, (src, dst) in enumerate(((wg_hbm, gate_w), (wu_hbm, up_w)))
    ]
    down_load = pltpu.make_async_copy(wd_hbm, down_in, local_sem.at[6])
    for load in loads + own_loads + [down_load]:
        load.start()
    pl.semaphore_wait(barrier, len(greeted))

    def remote(src, dst, send, recv, device):
        return pltpu.make_async_remote_copy(
            src_ref=src, dst_ref=dst, send_sem=send, recv_sem=recv, device_id=device, device_id_type=MESH
        )

    low, high = (pl.ds(0, HALF), pl.ds(rows - HALF, HALF))
    into_low, into_high = (pl.ds(0, HALF), pl.ds(HALF + rows, HALF))
    halos = []
    for i, (src, dst) in enumerate(((k_hbm, k_all), (v_hbm, v_all))):
        halos.append(
            remote(src.at[high], dst.at[into_low], halo_send.at[i, 0], halo_recv.at[i, 0], after)
        )
        halos.append(
            remote(src.at[low], dst.at[into_high], halo_send.at[i, 1], halo_recv.at[i, 1], before)
        )
    halos.append(
        remote(
            doc_row_hbm.at[:, high], doc_all.at[:, into_low], halo_send.at[2, 0], halo_recv.at[2, 0], after
        )
    )
    halos.append(
        remote(
            doc_row_hbm.at[:, low], doc_all.at[:, into_high], halo_send.at[2, 1], halo_recv.at[2, 1], before
        )
    )
    for halo in halos:
        halo.start()

    part_rows = depth // 2
    pieces = (
        (wg_hbm, gate_w, 0, depth),
        (wu_hbm, up_w, 0, depth),
        (None, down_w, 0, part_rows),
        (None, down_w, part_rows, part_rows),
    )

    def place(piece, chip_id, core_id):
        _, buf, first, count = pieces[piece]
        start = pl.multiple_of((chip_id * CORES + core_id) * depth + first, count)
        return buf.at[pl.ds(start, count)]

    def own(piece):
        src, _, first, count = pieces[piece]
        if src is None:
            return place(piece, chip, core)
        return src.at[pl.ds(first, count)]

    def ring_out(way, piece, distance):
        steps = -(distance - 1) if way == 0 else distance - 1
        dst = place(piece, chip_at(steps), core)
        src = own(piece) if distance == 1 else dst
        return remote(
            src,
            dst,
            ring_send.at[way, piece, distance],
            ring_recv.at[way, piece, distance],
            forward if way == 0 else backward,
        )

    def ring_in(way, piece, distance):
        dst = place(piece, chip_at(-distance if way == 0 else distance), core)
        return remote(
            dst,
            dst,
            ring_send.at[way, piece, distance],
            ring_recv.at[way, piece, distance],
            backward if way == 0 else forward,
        )

    def pair(way, piece, distance, core_id):
        steps = 0 if distance == 0 else (-distance if way == 0 else distance)
        dst = place(piece, chip_at(steps), core_id)
        src = own(piece) if distance == 0 else dst
        return remote(
            src, dst, pair_send.at[way, piece, distance], pair_recv.at[way, piece, distance], partner
        )

    def pair_in(way, piece, distance):
        steps = 0 if distance == 0 else (-distance if way == 0 else distance)
        dst = place(piece, chip_at(steps), 1 - core)
        return remote(
            dst, dst, pair_send.at[way, piece, distance], pair_recv.at[way, piece, distance], partner
        )

    sent = []

    def launch(copy):
        copy.start()
        sent.append(copy)

    rounds = []
    for both in ((0, 1), (2, 3)):
        for distance in range(1, half_ring + 1):
            rounds.append((distance, both[0], both[1]))
            if distance < half_ring:
                rounds.append((distance, both[1], both[0]))
    legs = [set(), set()]
    for distance, first, second in rounds:
        legs[0].add((distance, first))
        legs[1].add((distance, second))
    per_phase = len(rounds) // 2

    def pump(index):
        distance, first, second = rounds[index]
        for way, piece in ((0, first), (1, second)):
            ring_in(way, piece, distance).wait_recv()
            if (distance + 1, piece) in legs[way]:
                launch(ring_out(way, piece, distance + 1))
            launch(pair(way, piece, distance, core))
        if index == per_phase - 2:
            launch(ring_out(0, 2, 1))
            launch(ring_out(1, 3, 1))
        if index == per_phase - 1:
            launch(ring_out(0, 3, 1))
            launch(ring_out(1, 2, 1))

    launch(ring_out(0, 0, 1))
    launch(ring_out(1, 1, 1))
    launch(ring_out(0, 1, 1))
    launch(ring_out(1, 0, 1))
    for piece in (0, 1):
        launch(pair(0, piece, 0, core))
    down_load.wait()
    down_w[pl.ds(mine, depth), :] = down_in[...].T

    for load in loads[:3]:
        load.wait()
    for halo in halos:
        halo.wait_recv()
    span = rows + 2 * HALF
    at = lax.broadcasted_iota(jnp.int32, (1, span), 1) + (sp * rows - HALF)
    inside = jnp.logical_and(at >= 0, at < sp_size * rows)
    doc_keys = jnp.where(inside, doc_all[...], -1)
    reach = 3 * HALF
    offset = lax.broadcasted_iota(jnp.int32, (HALF, reach), 1) - lax.broadcasted_iota(
        jnp.int32, (HALF, reach), 0
    )
    near = jnp.logical_and(offset >= 0, offset <= 2 * HALF)
    for block in range(rows // HALF):
        doc_row = doc_all[:, (block + 1) * HALF : (block + 2) * HALF]
        doc_query = jnp.broadcast_to(doc_row, (HALF, HALF)).T
        same = jnp.concatenate([doc_query] * 3, 1) == doc_keys[:, block * HALF : block * HALF + reach]
        allowed = jnp.logical_and(near, same)
        for group in range(kv_local):
            lanes = slice(group * HEAD, (group + 1) * HEAD)
            key_blk = k_all[block * HALF : block * HALF + reach, lanes]
            value_blk = v_all[block * HALF : block * HALF + reach, lanes]
            for r in range(repeat):
                h = group * repeat + r
                query_blk = q_ref[block * HALF : (block + 1) * HALF, h * HEAD : (h + 1) * HEAD]
                scores = lax.dot_general(
                    query_blk, key_blk, (((1,), (1,)), ((), ())), preferred_element_type=jnp.float32
                ) * HEAD ** (-0.5)
                scores = jnp.where(allowed, scores, NEGATIVE)
                sink = jnp.full((1, 1), sink_ref[h], jnp.float32)
                top = jnp.maximum(jnp.max(scores, -1, keepdims=True), sink)
                weights = jnp.exp(scores - top)
                total = jnp.sum(weights, -1, keepdims=True) + jnp.exp(sink - top)
                summed = jnp.dot(
                    weights.astype(jnp.bfloat16), value_blk, preferred_element_type=jnp.float32
                )
                att[block * HALF : (block + 1) * HALF, h * HEAD : (h + 1) * HEAD] = (
                    summed / total
                ).astype(jnp.bfloat16)

    for piece in (2, 3):
        launch(pair(0, piece, 0, core))

    my_rows = pl.ds(pl.multiple_of(tp * token_rows, token_rows), token_rows)
    tokens[pl.ds(tp, 1)] = att[my_rows, :][None]
    pump(0)
    for i, j in enumerate(peers):
        launch(
            remote(
                att.at[pl.ds(pl.multiple_of(j * token_rows, token_rows), token_rows)],
                tokens.at[tp],
                tok_send.at[i],
                tok_recv.at[i],
                (sp, j),
            )
        )
    loads[3].wait()
    for i in range(tp_size - 1):
        source = lax.rem(tp + (tp_size - 1 - i), tp_size)
        slot = tokens.at[source]
        remote(slot, slot, tok_send.at[i], tok_recv.at[i], (sp, source)).wait_recv()
    tile = min(512, width)

    @pl.loop(0, width // tile)
    def _(t):
        lanes = pl.ds(pl.multiple_of(t * tile, tile), tile)
        mixed = ALPHA * res_ref[:, lanes].astype(jnp.float32)
        for j in range(tp_size):
            mixed += jnp.dot(
                tokens[j],
                w_out[j * cols_tp : (j + 1) * cols_tp, lanes],
                preferred_element_type=jnp.float32,
            )
        pre[:, lanes] = mixed

    strip = math.gcd(32, token_rows)

    @pl.loop(0, token_rows // strip)
    def _(t):
        here = pl.ds(pl.multiple_of(t * strip, strip), strip)
        there = pl.ds(pl.multiple_of(tp * token_rows + t * strip, strip), strip)
        normed[there, :] = layer_norm(pre[here, :], gain_one_ref[...]).astype(jnp.bfloat16)

    pump(1)
    for i, j in enumerate(peers):
        launch(
            remote(
                normed.at[my_rows], normed.at[my_rows], norm_send.at[i], norm_recv.at[i], (sp, j)
            )
        )
    for index in range(2, per_phase):
        pump(index)

    for load in own_loads:
        load.wait()
    for piece in (0, 1):
        pair_in(0, piece, 0).wait_recv()
    for distance, first, second in rounds[:per_phase]:
        pair_in(0, first, distance).wait_recv()
        pair_in(1, second, distance).wait_recv()
    for i in range(tp_size - 1):
        source = lax.rem(tp + (tp_size - 1 - i), tp_size)
        slot = normed.at[pl.ds(pl.multiple_of(source * token_rows, token_rows), token_rows)]
        remote(slot, slot, norm_send.at[i], norm_recv.at[i], (sp, source)).wait_recv()

    units = wg_hbm.shape[1]
    block_units = 256 if units % 256 == 0 else 128
    steps = units // block_units

    def hidden_tiles(first, last):
        @pl.loop(first, last)
        def _(t):
            lanes = pl.ds(pl.multiple_of(t * block_units, block_units), block_units)
            gate = jnp.dot(normed[...], gate_w[:, lanes], preferred_element_type=jnp.float32)
            up = jnp.dot(normed[...], up_w[:, lanes], preferred_element_type=jnp.float32)
            hidden[:, lanes] = (gate / (1.0 + jnp.exp(-gate)) * up).astype(jnp.bfloat16)

    middle = steps // 2
    hidden_tiles(0, middle)
    pump(per_phase)
    hidden_tiles(middle, steps)
    pump(per_phase + 1)

    chunk = CORES * depth
    order = []

    def chunk_sends(number, owner):
        lanes = pl.ds(pl.multiple_of(owner * chunk, chunk), chunk)
        for i, j in enumerate(peers):
            launch(
                remote(
                    parts.at[j, :, lanes],
                    others.at[i, :, lanes],
                    sum_send.at[number, i],
                    sum_recv.at[number, i],
                    (sp, j),
                )
            )

    def down_chunk(owner):
        start = pl.multiple_of(owner * chunk, chunk)
        part = lax.dot_general(
            hidden[...],
            down_w[pl.ds(start, chunk), :],
            (((1,), (1,)), ((), ())),
            preferred_element_type=jnp.float32,
        ).astype(jnp.bfloat16)
        for j in range(tp_size):
            parts[j, :, pl.ds(start, chunk)] = part[j * token_rows : (j + 1) * token_rows, :]
        order.append(owner)
        if len(order) > 1:
            chunk_sends(len(order) - 2, order[-2])

    for piece in (2, 3):
        pair_in(0, piece, 0).wait_recv()
    down_chunk(chip_at(0))
    index = per_phase + 2
    for distance in range(1, half_ring + 1):
        if distance == half_ring:
            pump(index)
            index += 1
            pair_in(0, 2, distance).wait_recv()
            pair_in(1, 3, distance).wait_recv()
            down_chunk(chip_at(distance))
            continue
        if distance > 1:
            pump(index)
            pump(index + 1)
            index += 2
        for piece in (2, 3):
            pair_in(0, piece, distance).wait_recv()
            pair_in(1, piece, distance).wait_recv()
        down_chunk(chip_at(-distance))
        down_chunk(chip_at(distance))
    chunk_sends(len(order) - 1, order[-1])
    for number, owner in enumerate(order):
        lanes = pl.ds(pl.multiple_of(owner * chunk, chunk), chunk)
        for i in range(tp_size - 1):
            source = lax.rem(tp + (tp_size - 1 - i), tp_size)
            slot = others.at[i, :, lanes]
            remote(slot, slot, sum_send.at[number, i], sum_recv.at[number, i], (sp, source)).wait_recv()

    @pl.loop(0, token_rows // strip)
    def _(t):
        here = pl.ds(pl.multiple_of(t * strip, strip), strip)
        there = pl.ds(pl.multiple_of(tp * token_rows + t * strip, strip), strip)
        down = parts[pl.ds(tp, 1), here, :][0].astype(jnp.float32)
        for i in range(tp_size - 1):
            down += others[i, here, :].astype(jnp.float32)
        pre_two = ALPHA * normed[there, :].astype(jnp.float32) + down
        out_ref[here, :] = layer_norm(pre_two, gain_two_ref[...]).astype(jnp.bfloat16)

    for halo in halos:
        halo.wait_send()
    for copy in sent:
        copy.wait_send()


def solution(mesh):
    sp_size = mesh.shape["sp"]
    tp_size = mesh.shape["tp"]

    def per_device(
        queries,
        keys,
        values,
        doc_ids,
        sink_logit,
        residual_in,
        w_out,
        gain_one,
        w_gate,
        w_up,
        w_down,
        gain_two,
    ):
        rows = queries.shape[0]
        token_rows, width = residual_in.shape
        units = w_gate.shape[1]
        span = rows + 2 * HALF
        chips = sp_size // CORES
        full = w_gate.shape[0] * sp_size
        bf16, f32 = (jnp.bfloat16, jnp.float32)
        dma = pltpu.SemaphoreType.DMA
        others = max(tp_size - 1, 1)
        vmem, anywhere = (pl.BlockSpec(memory_space=pltpu.VMEM), pl.BlockSpec(memory_space=pl.ANY))
        return pl.pallas_call(
            functools.partial(kernel, sp_size, tp_size),
            out_shape=jax.ShapeDtypeStruct((token_rows, width), bf16),
            in_specs=[vmem, pl.BlockSpec(memory_space=pltpu.SMEM)] + [vmem] * 3 + [anywhere] * 7,
            out_specs=vmem,
            scratch_shapes=[
                pltpu.VMEM((span, keys.shape[1]), bf16),
                pltpu.VMEM((span, keys.shape[1]), bf16),
                pltpu.VMEM((1, span), jnp.int32),
                pltpu.VMEM(w_out.shape, bf16),
                pltpu.VMEM((full, units), bf16),
                pltpu.VMEM((full, units), bf16),
                pltpu.VMEM((w_down.shape[1] * sp_size, units), bf16),
                pltpu.VMEM((rows, queries.shape[1]), bf16),
                pltpu.VMEM((tp_size, token_rows, queries.shape[1]), bf16),
                pltpu.VMEM((token_rows, width), f32),
                pltpu.VMEM((rows, width), bf16),
                pltpu.VMEM((rows, units), bf16),
                pltpu.VMEM(w_down.shape, bf16),
                pltpu.VMEM((tp_size, token_rows, width), bf16),
                pltpu.VMEM((others, token_rows, width), bf16),
                dma((7,)),
                dma((3, 2)),
                dma((3, 2)),
                dma((2, 4, chips // 2 + 1)),
                dma((2, 4, chips // 2 + 1)),
                dma((2, 4, chips // 2 + 1)),
                dma((2, 4, chips // 2 + 1)),
                dma((others,)),
                dma((others,)),
                dma((others,)),
                dma((others,)),
                dma((chips, others)),
                dma((chips, others)),
            ],
            compiler_params=pltpu.CompilerParams(
                collective_id=0, has_side_effects=True, vmem_limit_bytes=62 * 2**20
            ),
        )(
            queries,
            sink_logit,
            residual_in,
            gain_one[None, :],
            gain_two[None, :],
            keys,
            values,
            doc_ids[None, :],
            w_out,
            w_gate,
            w_up,
            w_down,
        )

    in_specs = (
        P("sp", "tp"),
        P("sp", "tp"),
        P("sp", "tp"),
        P("sp"),
        P("tp"),
        P(("sp", "tp"), None),
        P(),
        P(),
        P("sp", "tp"),
        P("sp", "tp"),
        P("tp", "sp"),
        P(),
    )
    return jax.shard_map(
        per_device, mesh=mesh, in_specs=in_specs, out_specs=P(("sp", "tp"), None), check_vma=False
    )
```

profile of v0, /device:TPU:1, one launch (start us, length us, event | category | flops | bytes accessed | tf_op | source)
XLA Modules:
  0.0 132.7 jit_solution(17228693477554036002)
XLA Ops:
  0.0 1.8 %copy.13.wd_hbm = bf16[1408,64]{1,0:T(8,128)(2,1)} copy(bf16[1408,64]{0,1:T(8,128)(2,1)} %param.22) | data formatting | bytes 360448 | tf_op args[10]
  1.8 129.0 %shard_map.118 = bf16[128,2048]{1,0:T(8,128)(2,1)} custom-call(bf16[512,256]{1,0:T(8,128)(2,1)} %q_ref.1, f32[2]{0:T(128)} %sink_ref.1, bf16[128,2048]{1,0:T(8,128)(2,1)} %res_ref.1, f32[1,2048]{1,0:T(1,128)} %bitcast.3, f32[1,2048]{1,0:T(1,128)} %bitcast.4, bf16[512,128]{1,0:T(8,128)(2,1)} %k_hbm.1, bf16[512,128]{1,0:T(8,128)(2,1)} %v_hbm.1, ...), custom_call_target="tpu_custom_call" | custom-call | tf_op jit(solution)/shard_map/pallas_call | solution.py:480
  130.8 1.9 %copy.15 = bf16[128,2048]{1,0:T(8,128)(2,1)} copy(bf16[128,2048]{1,0:T(8,128)(2,1)} %shard_map.118) | data formatting | bytes 1048576
where the time goes:
time: 133 us
  Pallas kernels  129 us (97%)
  local copies, waits for them, and re-layouts  3.71 us (3%)
    pallas_call x1, Pallas kernels, per_device(): pl.pallas_call(functools.partial(kernel, sp_size, tp_size), out_shape=jax...  129 us
    unnamed x2, local copies, waits for them, and re-layouts  3.71 us

commit v1 on v0

v1 whole, which is shorter than its diff:
```python
import functools

import jax
import jax.numpy as jnp
from jax import lax
from jax.experimental import pallas as pl
from jax.experimental.pallas import tpu as pltpu
from jax.sharding import PartitionSpec as P

HEAD = 128
HALF = 128
CORES = 2
SIDE = 4
CHIPS = SIDE * SIDE
FAR = CHIPS // 2
TP = 4
ALPHA = 2.0**0.5
EPS = 1e-05
NEGATIVE = -1e30
MESH = pl.DeviceIdType.MESH
BF16 = jnp.bfloat16
F32 = jnp.float32
SEGMENTS = ((0, 16),)


def layer_norm(values_in, gain):
    average = jnp.mean(values_in, -1, keepdims=True)
    centred = values_in - average
    variance = jnp.mean(centred * centred, -1, keepdims=True)
    return centred * lax.rsqrt(variance + EPS) * gain


def slot_of(way, distance):
    if distance == 0:
        return 0
    if distance == FAR:
        return CHIPS - 1
    return 2 * distance - 1 + way


def kernel(
    sink_ref,
    q_hbm,
    res_hbm,
    gain_one_hbm,
    gain_two_hbm,
    k_hbm,
    v_hbm,
    doc_hbm,
    w_out_hbm,
    wg_hbm,
    wu_hbm,
    wd_hbm,
    out_ref,
    q_all,
    k_all,
    v_all,
    doc_all,
    gain_one,
    gain_two,
    w_out,
    gate_w,
    up_w,
    down_w,
    att_all,
    res_all,
    pre,
    normed,
    normed_a,
    normed_b,
    gate_acc,
    up_acc,
    hidden,
    parts,
    relay_m,
    relay_p,
    in_m,
    in_p,
    local_sem,
    halo_send,
    halo_recv,
    ring_send,
    ring_recv,
    pair_send,
    pair_recv,
    res_send,
    res_recv,
    att_send,
    att_recv,
    sum_send,
    sum_recv,
):
    sp = lax.axis_index("sp")
    tp = lax.axis_index("tp")
    sp_size = CHIPS * CORES
    core = lax.rem(sp, CORES)
    chip = sp // CORES
    my_y = lax.rem(chip, SIDE)
    my_z = chip // SIDE
    turn = lax.rem(my_y + my_z, SIDE)
    pos = (my_z * SIDE + turn, my_y * SIDE + turn)

    def chip_at(ring, steps):
        p = lax.rem(pos[ring] + (CHIPS + steps), CHIPS)
        a = p // SIDE
        b = lax.rem(lax.rem(p, SIDE) + (SIDE - a), SIDE)
        return a * SIDE + b if ring == 0 else b * SIDE + a

    def chip_of_slot(ring, slot):
        return chip_at(ring, slot // 2 if slot % 2 == 0 else -((slot + 1) // 2))

    rows = q_hbm.shape[0]
    token_rows = res_hbm.shape[0]
    depth = wg_hbm.shape[0]
    units = wg_hbm.shape[1]
    width = res_hbm.shape[1]
    sub_rows = depth // 2
    wide = CORES * depth

    ring_next = [[chip_at(ring, 1) * CORES + core, chip_at(ring, -1) * CORES + core] for ring in range(2)]
    mixed_next = [
        ring_next[0][way] * (1 - core) + ring_next[1][way] * core for way in range(2)
    ]
    partner = (chip * CORES + (1 - core), tp)
    after = (lax.rem(sp + 1, sp_size), tp)
    before = (lax.rem(sp + sp_size - 1, sp_size), tp)
    tp_right = lax.rem(tp + 1, TP)
    tp_left = lax.rem(tp + TP - 1, TP)
    tp_far = lax.rem(tp + 2, TP)
    sides = [(sp, tp_right), (sp, tp_left)]
    from_side = [tp_left, tp_right]

    barrier = pltpu.get_barrier_semaphore()
    greeted = [(ring_next[ring][way], tp) for ring in range(2) for way in range(2)]
    greeted += [partner, after, before] + sides
    for device in greeted:
        pl.semaphore_signal(barrier, inc=1, device_id=device, device_id_type=MESH)

    own_rows = pl.ds(pl.multiple_of(core * depth, depth), depth)
    loads = [
        pltpu.make_async_copy(k_hbm, k_all.at[pl.ds(HALF, rows)], local_sem.at[0]),
        pltpu.make_async_copy(v_hbm, v_all.at[pl.ds(HALF, rows)], local_sem.at[1]),
        pltpu.make_async_copy(doc_hbm, doc_all.at[:, pl.ds(HALF, rows)], local_sem.at[2]),
        pltpu.make_async_copy(q_hbm, q_all, local_sem.at[3]),
    ]
    out_loads = [
        pltpu.make_async_copy(w_out_hbm, w_out, local_sem.at[4]),
        pltpu.make_async_copy(res_hbm, res_all.at[tp], local_sem.at[5]),
        pltpu.make_async_copy(gain_one_hbm, gain_one, local_sem.at[6]),
        pltpu.make_async_copy(gain_two_hbm, gain_two, local_sem.at[7]),
    ]
    own_loads = [
        pltpu.make_async_copy(src, dst.at[own_rows], local_sem.at[8 + i])
        for i, (src, dst) in enumerate(((wg_hbm, gate_w), (wu_hbm, up_w), (wd_hbm, down_w)))
    ]
    for load in loads + out_loads + own_loads:
        load.start()
    pl.semaphore_wait(barrier, len(greeted))

    def remote(src, dst, send, recv, device):
        return pltpu.make_async_remote_copy(
            src_ref=src, dst_ref=dst, send_sem=send, recv_sem=recv, device_id=device, device_id_type=MESH
        )

    sent = []

    def launch(copy):
        copy.start()
        sent.append(copy)

    def arrive(copy):
        copy.wait_recv()

    low, high = (pl.ds(0, HALF), pl.ds(rows - HALF, HALF))
    into_low, into_high = (pl.ds(0, HALF), pl.ds(HALF + rows, HALF))
    halos = []
    for i, (src, dst) in enumerate(((k_hbm, k_all), (v_hbm, v_all))):
        halos.append(
            remote(src.at[high], dst.at[into_low], halo_send.at[i, 0], halo_recv.at[i, 0], after)
        )
        halos.append(
            remote(src.at[low], dst.at[into_high], halo_send.at[i, 1], halo_recv.at[i, 1], before)
        )
    halos.append(
        remote(doc_hbm.at[:, high], doc_all.at[:, into_low], halo_send.at[2, 0], halo_recv.at[2, 0], after)
    )
    halos.append(
        remote(doc_hbm.at[:, low], doc_all.at[:, into_high], halo_send.at[2, 1], halo_recv.at[2, 1], before)
    )
    for halo in halos:
        launch(halo)

    sources = (wg_hbm, wu_hbm, wd_hbm)
    buffers = (gate_w, up_w, down_w)

    def place(piece, way, distance, core_id):
        start = slot_of(way, distance) * wide + core_id * depth + (piece % 2) * sub_rows
        return buffers[piece // 2].at[pl.ds(pl.multiple_of(start, sub_rows), sub_rows)]

    def own(piece):
        return sources[piece // 2].at[pl.ds((piece % 2) * sub_rows, sub_rows)]

    def ring_to(piece, way):
        kind = piece // 2
        return (ring_next[kind][way] if kind < 2 else mixed_next[way], tp)

    def ring_out(way, piece, distance):
        src = own(piece) if distance == 1 else place(piece, way, distance - 1, core)
        return remote(
            src,
            place(piece, way, distance, core),
            ring_send.at[way, piece, distance],
            ring_recv.at[way, piece, distance],
            ring_to(piece, way),
        )

    def ring_in(way, piece, distance):
        dst = place(piece, way, distance, core)
        return remote(
            dst,
            dst,
            ring_send.at[way, piece, distance],
            ring_recv.at[way, piece, distance],
            ring_to(piece, 1 - way),
        )

    def pair_out(way, piece, distance):
        dst = place(piece, way, distance, core)
        src = own(piece) if distance == 0 else dst
        return remote(
            src, dst, pair_send.at[way, piece, distance], pair_recv.at[way, piece, distance], partner
        )

    def pair_in(way, piece, distance):
        dst = place(piece, way, distance, 1 - core)
        return remote(
            dst, dst, pair_send.at[way, piece, distance], pair_recv.at[way, piece, distance], partner
        )

    rounds = []
    for distance in range(1, FAR + 1):
        rounds.append((distance, 0, 1))
        if distance < FAR:
            rounds.append((distance, 1, 0))
    per_phase = len(rounds)

    def pump(index):
        if index < per_phase:
            bases = (0, 2)
        else:
            bases = (4,)
        distance, first, second = rounds[index % per_phase]
        for base in bases:
            for way, sub in ((0, first), (1, second)):
                piece = base + sub
                arrive(ring_in(way, piece, distance))
                if distance + 1 < FAR or (distance + 1 == FAR and sub == way):
                    launch(ring_out(way, piece, distance + 1))
                launch(pair_out(way, piece, distance))
        if index == per_phase - 2:
            launch(ring_out(0, 4, 1))
            launch(ring_out(1, 5, 1))
        if index == per_phase - 1:
            launch(ring_out(0, 5, 1))
            launch(ring_out(1, 4, 1))

    for first, second in ((0, 1), (1, 0)):
        for base in (0, 2):
            launch(ring_out(0, base + first, 1))
            launch(ring_out(1, base + second, 1))

    def res_half(half):
        return pl.ds(half * (token_rows // 2), token_rows // 2)

    def res_own(way, k):
        half = res_half(k if way == 0 else 1 - k)
        return remote(
            res_hbm.at[half], res_all.at[tp, half], res_send.at[way, k], res_recv.at[way, k], sides[way]
        )

    def res_in(way, k):
        half = res_half((k if way == 0 else 1 - k) if k < 2 else way)
        slot = res_all.at[from_side[way] if k < 2 else tp_far, half]
        return remote(slot, slot, res_send.at[way, k], res_recv.at[way, k], sides[1 - way])

    def res_forward(way):
        slot = res_all.at[from_side[way], res_half(way)]
        return remote(slot, slot, res_send.at[way, 2], res_recv.at[way, 2], sides[way])

    for k in range(2):
        for way in range(2):
            launch(res_own(way, k))
    for piece in range(6):
        launch(pair_out(0, piece, 0))

    def block_rows(block):
        return pl.ds(block * HALF, HALF)

    def att_copy(way, block, source, index, device):
        slot = att_all.at[source, block_rows(block)]
        return remote(slot, slot, att_send.at[way, index], att_recv.at[way, index], device)

    for load in loads:
        load.wait()
    for halo in halos:
        arrive(halo)
    span = rows + 2 * HALF
    at = lax.broadcasted_iota(jnp.int32, (1, span), 1) + (sp * rows - HALF)
    inside = jnp.logical_and(at >= 0, at < sp_size * rows)
    doc_keys = jnp.where(inside, doc_all[...], -1)
    reach = 3 * HALF
    repeat = q_hbm.shape[1] // HEAD
    offset = lax.broadcasted_iota(jnp.int32, (HALF, reach), 1) - lax.broadcasted_iota(
        jnp.int32, (HALF, reach), 0
    )
    near = jnp.logical_and(offset >= 0, offset <= 2 * HALF)

    def attend(block):
        doc_row = doc_all[:, (block + 1) * HALF : (block + 2) * HALF]
        doc_query = jnp.broadcast_to(doc_row, (HALF, HALF)).T
        same = jnp.concatenate([doc_query] * 3, 1) == doc_keys[:, block * HALF : block * HALF + reach]
        allowed = jnp.logical_and(near, same)
        key_blk = k_all[block * HALF : block * HALF + reach, :]
        value_blk = v_all[block * HALF : block * HALF + reach, :]
        for h in range(repeat):
            query_blk = q_all[block * HALF : (block + 1) * HALF, h * HEAD : (h + 1) * HEAD]
            scores = lax.dot_general(
                query_blk, key_blk, (((1,), (1,)), ((), ())), preferred_element_type=F32
            ) * HEAD ** (-0.5)
            scores = jnp.where(allowed, scores, NEGATIVE)
            sink = jnp.full((1, 1), sink_ref[h], F32)
            top = jnp.maximum(jnp.max(scores, -1, keepdims=True), sink)
            weights = jnp.exp(scores - top)
            total = jnp.sum(weights, -1, keepdims=True) + jnp.exp(sink - top)
            summed = jnp.dot(weights.astype(BF16), value_blk, preferred_element_type=F32)
            att_all[pl.ds(tp, 1), block * HALF : (block + 1) * HALF, h * HEAD : (h + 1) * HEAD] = (
                summed / total
            ).astype(BF16)[None]
        for way in range(2):
            launch(att_copy(way, block, tp, block, sides[way]))

    def att_forward(block):
        way = block % 2
        arrive(att_copy(way, block, from_side[way], block, sides[1 - way]))
        launch(att_copy(way, block, from_side[way], 4 + block // 2, sides[way]))

    def att_rest(block):
        way = block % 2
        arrive(att_copy(1 - way, block, from_side[1 - way], block, sides[way]))
        arrive(att_copy(way, block, tp_far, 4 + block // 2, sides[1 - way]))

    tile = 512
    strip = 32

    def project(block):
        @pl.loop(0, width // tile)
        def _(t):
            lanes = pl.ds(pl.multiple_of(t * tile, tile), tile)
            mixed = ALPHA * res_all[block, :, lanes].astype(F32)
            for j in range(TP):
                mixed += jnp.dot(
                    att_all[j, block * HALF : (block + 1) * HALF, :],
                    w_out[j * 256 : (j + 1) * 256, lanes],
                    preferred_element_type=F32,
                )
            pre[:, lanes] = mixed

        @pl.loop(0, token_rows // strip)
        def _(t):
            here = pl.ds(pl.multiple_of(t * strip, strip), strip)
            there = pl.ds(pl.multiple_of(block * HALF + t * strip, strip), strip)
            normed[there, :] = layer_norm(pre[here, :], gain_one[...]).astype(BF16)

        part = slice(block * HALF, (block + 1) * HALF)
        for slot in range(CHIPS):
            to = slice(slot * wide, (slot + 1) * wide)
            for ring, buf in ((0, normed_a), (1, normed_b)):
                lanes = pl.ds(pl.multiple_of(chip_of_slot(ring, slot) * wide, wide), wide)
                buf[part, to] = normed[part, lanes]

    def gate_up(lo, hi, lanes):
        deep = slice(lo * wide, hi * wide)
        gate = jnp.dot(normed_a[:, deep], gate_w[deep, lanes], preferred_element_type=F32)
        up = jnp.dot(normed_b[:, deep], up_w[deep, lanes], preferred_element_type=F32)
        if lo > 0:
            gate += gate_acc[:, lanes]
            up += up_acc[:, lanes]
        if hi < CHIPS:
            gate_acc[:, lanes] = gate
            up_acc[:, lanes] = up
        else:
            hidden[:, lanes] = (gate / (1.0 + jnp.exp(-gate)) * up).astype(BF16)

    def gate_up_tiles(lo, hi, first, last):
        @pl.loop(first, last)
        def _(t):
            gate_up(lo, hi, pl.ds(pl.multiple_of(t * 256, 256), 256))

    def gate_up_rest(lo, hi):
        gate_up(lo, hi, slice(units // 256 * 256, units))

    def pair_weights(kind, distance):
        for sub in range(2):
            piece = 2 * kind + sub
            if distance == FAR:
                arrive(pair_in(sub, piece, distance))
            elif distance == 0:
                arrive(pair_in(0, piece, 0))
            else:
                for way in range(2):
                    arrive(pair_in(way, piece, distance))

    def rows_of(j):
        return pl.ds(pl.multiple_of(j * token_rows, token_rows), token_rows)

    def down_chunk(k):
        part = lax.dot_general(
            hidden[...],
            down_w[2 * k * wide : 2 * (k + 1) * wide, :],
            (((1,), (1,)), ((), ())),
            preferred_element_type=F32,
        ).astype(BF16)
        parts[2 * k] = part[:, :wide]
        parts[2 * k + 1] = part[:, wide:]
        a, b = 2 * k, 2 * k + 1
        far = rows_of(tp_far)
        launch(remote(parts.at[a, far], relay_m.at[k], sum_send.at[0, k, 0], sum_recv.at[0, k, 0], sides[0]))
        launch(remote(parts.at[b, far], relay_p.at[k], sum_send.at[1, k, 0], sum_recv.at[1, k, 0], sides[1]))
        launch(
            remote(
                parts.at[b, rows_of(tp_right)], in_m.at[b], sum_send.at[0, k, 1], sum_recv.at[0, k, 1], sides[0]
            )
        )
        launch(
            remote(
                parts.at[a, rows_of(tp_left)], in_p.at[a], sum_send.at[1, k, 1], sum_recv.at[1, k, 1], sides[1]
            )
        )

    def sum_in(way, slot, k, index):
        return remote(slot, slot, sum_send.at[way, k, index], sum_recv.at[way, k, index], sides[1 - way])

    def relay_chunk(k):
        a, b = 2 * k, 2 * k + 1
        for way, slot, held, j, target in (
            (0, a, relay_m, tp_right, in_m),
            (1, b, relay_p, tp_left, in_p),
        ):
            arrive(sum_in(way, held.at[k], k, 0))
            here = rows_of(j)
            parts[slot, here, :] = (
                parts[slot, here, :].astype(F32) + held[k].astype(F32)
            ).astype(BF16)
            launch(
                remote(
                    parts.at[slot, here],
                    target.at[slot],
                    sum_send.at[way, k, 2],
                    sum_recv.at[way, k, 2],
                    sides[way],
                )
            )

    first_lanes = lax.broadcasted_iota(jnp.int32, (token_rows, wide), 1) < depth

    def finish_chunk(k):
        a, b = 2 * k, 2 * k + 1
        arrive(sum_in(0, in_m.at[b], k, 1))
        arrive(sum_in(1, in_p.at[a], k, 1))
        arrive(sum_in(0, in_m.at[a], k, 2))
        arrive(sum_in(1, in_p.at[b], k, 2))
        for slot in (a, b):
            down = (
                parts[slot, rows_of(tp), :].astype(F32)
                + in_m[slot].astype(F32)
                + in_p[slot].astype(F32)
            )
            for ring in range(2):
                lanes = pl.ds(pl.multiple_of(chip_of_slot(ring, slot) * wide, wide), wide)
                mine = first_lanes if ring == 0 else jnp.logical_not(first_lanes)
                pre[:, lanes] += jnp.where(mine, down, 0.0)

    for block in range(4):
        attend(block)
        pump(block)
    for way in range(2):
        arrive(res_in(way, 0))
        launch(res_forward(way))
    pump(4)
    pump(5)
    pump(6)
    for block in range(4):
        att_forward(block)
    pump(7)
    pump(8)
    for load in out_loads:
        load.wait()
    for way in range(2):
        arrive(res_in(way, 1))
        arrive(res_in(way, 2))
    for block in range(4):
        att_rest(block)
        project(block)
        pump(9 + block)
    pre[...] = ALPHA * normed[rows_of(tp), :].astype(F32)
    pump(13)
    pump(14)
    for load in own_loads:
        load.wait()
    for kind in range(2):
        for distance in range(FAR + 1):
            pair_weights(kind, distance)
    gate_up_tiles(0, 16, 0, 2)
    pump(15)
    pump(16)
    gate_up_tiles(0, 16, 2, 4)
    pump(17)
    pump(18)
    gate_up_tiles(0, 16, 4, 5)
    gate_up_rest(0, 16)
    pump(19)
    pair_weights(2, 0)
    index = 20
    for k in range(FAR):
        while index < 2 * per_phase and rounds[index - per_phase][0] <= k + 1:
            pump(index)
            index += 1
        pair_weights(2, k + 1)
        down_chunk(k)
        if k >= 1:
            relay_chunk(k - 1)
        if k >= 3:
            finish_chunk(k - 3)
    relay_chunk(FAR - 1)
    for k in range(FAR - 3, FAR):
        finish_chunk(k)

    @pl.loop(0, token_rows // strip)
    def _(t):
        here = pl.ds(pl.multiple_of(t * strip, strip), strip)
        out_ref[here, :] = layer_norm(pre[here, :], gain_two[...]).astype(BF16)

    for copy in sent:
        copy.wait_send()


def solution(mesh):
    def per_device(
        queries,
        keys,
        values,
        doc_ids,
        sink_logit,
        residual_in,
        w_out,
        gain_one,
        w_gate,
        w_up,
        w_down,
        gain_two,
    ):
        rows = queries.shape[0]
        token_rows, width = residual_in.shape
        units = w_gate.shape[1]
        span = rows + 2 * HALF
        dma = pltpu.SemaphoreType.DMA
        vmem, anywhere = (pl.BlockSpec(memory_space=pltpu.VMEM), pl.BlockSpec(memory_space=pl.ANY))
        return pl.pallas_call(
            kernel,
            out_shape=jax.ShapeDtypeStruct((token_rows, width), BF16),
            in_specs=[pl.BlockSpec(memory_space=pltpu.SMEM)] + [anywhere] * 11,
            out_specs=vmem,
            scratch_shapes=[
                pltpu.VMEM(queries.shape, BF16),
                pltpu.VMEM((span, keys.shape[1]), BF16),
                pltpu.VMEM((span, keys.shape[1]), BF16),
                pltpu.VMEM((1, span), jnp.int32),
                pltpu.VMEM((1, width), F32),
                pltpu.VMEM((1, width), F32),
                pltpu.VMEM(w_out.shape, BF16),
                pltpu.VMEM((width, units), BF16),
                pltpu.VMEM((width, units), BF16),
                pltpu.VMEM((width, units), BF16),
                pltpu.VMEM((TP, rows, queries.shape[1]), BF16),
                pltpu.VMEM((TP, token_rows, width), BF16),
                pltpu.VMEM((token_rows, width), F32),
                pltpu.VMEM((rows, width), BF16),
                pltpu.VMEM((rows, width), BF16),
                pltpu.VMEM((rows, width), BF16),
                pltpu.VMEM((rows, units), F32),
                pltpu.VMEM((rows, units), F32),
                pltpu.VMEM((rows, units), BF16),
                pltpu.VMEM((CHIPS, rows, width // CHIPS), BF16),
                pltpu.VMEM((FAR, token_rows, width // CHIPS), BF16),
                pltpu.VMEM((FAR, token_rows, width // CHIPS), BF16),
                pltpu.VMEM((CHIPS, token_rows, width // CHIPS), BF16),
                pltpu.VMEM((CHIPS, token_rows, width // CHIPS), BF16),
                dma((11,)),
                dma((3, 2)),
                dma((3, 2)),
                dma((2, 6, FAR + 1)),
                dma((2, 6, FAR + 1)),
                dma((2, 6, FAR + 1)),
                dma((2, 6, FAR + 1)),
                dma((2, 3)),
                dma((2, 3)),
                dma((2, 6)),
                dma((2, 6)),
                dma((2, FAR, 3)),
                dma((2, FAR, 3)),
            ],
            compiler_params=pltpu.CompilerParams(
                collective_id=0, has_side_effects=True, vmem_limit_bytes=62 * 2**20
            ),
        )(
            sink_logit,
            queries,
            residual_in,
            gain_one[None, :],
            gain_two[None, :],
            keys,
            values,
            doc_ids[None, :],
            w_out,
            w_gate,
            w_up,
            w_down.T,
        )

    in_specs = (
        P("sp", "tp"),
        P("sp", "tp"),
        P("sp", "tp"),
        P("sp"),
        P("tp"),
        P(("sp", "tp"), None),
        P(),
        P(),
        P("sp", "tp"),
        P("sp", "tp"),
        P("tp", "sp"),
        P(),
    )
    return jax.shard_map(
        per_device, mesh=mesh, in_specs=in_specs, out_specs=P(("sp", "tp"), None), check_vma=False
    )
```

time: 133 us -> 99.8 us (0.75)
  Pallas kernels: 129 us -> 97.8 us
  local copies, waits for them, and re-layouts: 3.71 us -> 1.88 us
    pallas_call x1, Pallas kernels: 129 us -> 97.8 us  [per_device(): pl.pallas_call(kernel, out_shape=jax.ShapeDtypeStruct((token_rows, width)...]
    unnamed x2 -> x1, local copies, waits for them, and re-layouts: 3.71 us -> 1.88 us
where the time goes in v1:
time: 99.8 us; the launch traced here: 99.6 us
  Pallas kernels  97.8 us (98%)
  local copies, waits for them, and re-layouts  1.88 us (2%)
    pallas_call x1, Pallas kernels, per_device(): pl.pallas_call(kernel, out_shape=jax.ShapeDtypeStruct((token_rows, width)...  97.8 us

profile of v1, /device:TPU:1, one launch (start us, length us, event | category | flops | bytes accessed | tf_op | source)
XLA Modules:
  0.0 99.6 jit_solution(6650062548951667427)
XLA Ops:
  0.0 97.8 %shard_map.118 = bf16[128,2048]{1,0:T(8,128)(2,1)} custom-call(f32[2]{0:T(128)} %sink_ref.1, bf16[512,256]{1,0:T(8,128)(2,1)} %q_hbm.1, bf16[128,2048]{1,0:T(8,128)(2,1)} %res_hbm.1, f32[1,2048]{1,0:T(1,128)} %bitcast.5, f32[1,2048]{1,0:T(1,128)} %bitcast.6, bf16[512,128]{1,0:T(8,128)(2,1)} %k_hbm.1, bf16[512,128]{1,0:T(8,128)(2,1)} %v_hbm.1, ...), custom_call_target="tpu_custom_call" | custom-call | tf_op jit(solution)/shard_map/pallas_call | solution.py:568
  97.8 1.9 %copy.14 = bf16[128,2048]{1,0:T(8,128)(2,1)} copy(bf16[128,2048]{1,0:T(8,128)(2,1)} %shard_map.118) | data formatting | bytes 1048576

commit v2 on v1

v2 whole, which is shorter than its diff:
```python
import jax
import jax.numpy as jnp
from jax import lax
from jax.experimental import pallas as pl
from jax.experimental.pallas import tpu as pltpu
from jax.sharding import PartitionSpec as P

HEAD = 128
HALF = 128
CORES = 2
SIDE = 4
CHIPS = SIDE * SIDE
TP = 4
ALPHA = 2.0**0.5
EPS = 1e-05
NEGATIVE = -1e30
MESH = pl.DeviceIdType.MESH
BF16 = jnp.bfloat16
F32 = jnp.float32
OFFSETS = (
    (0, 0),
    (1, 0),
    (0, 1),
    (-1, 0),
    (0, -1),
    (1, 1),
    (-1, -1),
    (1, -1),
    (-1, 1),
    (2, 0),
    (0, 2),
    (2, 1),
    (1, 2),
    (2, -1),
    (-1, 2),
    (2, 2),
)
SLOT = {offset: slot for slot, offset in enumerate(OFFSETS)}
SEGMENTS = ((0, 5), (5, 11), (11, 16))
CHUNKS = ((1, 2), (3, 4), (5, 6), (7, 8), (9, 10), (11, 12), (13, 14), (0, 15))
LAST = 10


def message(number, way):
    s = 2 * way - 1
    return (
        None,
        (0, (0, 0), (s, 0), False),
        (1, (0, 0), (0, s), False),
        (0, (s, 0), (2, 0), True),
        (1, (s, 0), (s, s), False),
        (1, (-s, 0), (-s, s), False),
        (1, (0, s), (0, 2), True),
        (1, (2, 0), (2, s), False),
        (1, (s, s), (s, 2), True),
        (1, (-s, s), (-s, 2), True),
        (1, (2, s), (2, 2), True),
    )[number]


FOLLOW = {1: (3, 4, 5), 2: (6,), 3: (7,), 4: (8,), 5: (9,), 7: (10,)}


def segment_of(slot):
    return [lo <= slot < hi for lo, hi in SEGMENTS].index(True)


def chunk_of(slot):
    return [slot in chunk for chunk in CHUNKS].index(True)


def layer_norm(values_in, gain):
    average = jnp.mean(values_in, -1, keepdims=True)
    centred = values_in - average
    variance = jnp.mean(centred * centred, -1, keepdims=True)
    return centred * lax.rsqrt(variance + EPS) * gain


def kernel(
    sink_ref,
    q_hbm,
    res_hbm,
    gain_one_hbm,
    gain_two_hbm,
    k_hbm,
    v_hbm,
    doc_hbm,
    w_out_hbm,
    wg_hbm,
    wu_hbm,
    wd_hbm,
    out_ref,
    q_all,
    k_all,
    v_all,
    doc_all,
    gains_in,
    gains,
    res_all,
    w_out,
    gate_w,
    up_w,
    down_w,
    att,
    tokens,
    pre,
    normed,
    gate_acc,
    up_acc,
    hidden,
    parts,
    relays,
    arrived,
    local_sem,
    halo_send,
    halo_recv,
    ring_send,
    ring_recv,
    pair_send,
    pair_recv,
    down_recv,
    tok_send,
    tok_recv,
    norm_send,
    norm_recv,
    sum_send,
    relay_recv,
    sum_recv,
):
    sp = lax.axis_index("sp")
    tp = lax.axis_index("tp")
    sp_size = CHIPS * CORES
    core = lax.rem(sp, CORES)
    chip = sp // CORES
    my_y = lax.rem(chip, SIDE)
    my_z = chip // SIDE

    def chip_at(dz, dy):
        z = lax.rem(my_z + (dz + SIDE), SIDE)
        y = lax.rem(my_y + (dy + SIDE), SIDE)
        return z * SIDE + y

    rows = q_hbm.shape[0]
    token_rows = res_hbm.shape[0]
    depth = wg_hbm.shape[0]
    units = wg_hbm.shape[1]
    width = res_hbm.shape[1]
    sub_rows = depth // 2
    wide = CORES * depth
    half_rows = token_rows // 2

    def chip_lanes(slot):
        return pl.ds(pl.multiple_of(chip_at(*OFFSETS[slot]) * wide, wide), wide)

    def slot_lanes(slot):
        return slice(slot * wide, (slot + 1) * wide)

    along_z = [chip_at(1, 0) * CORES + core, chip_at(-1, 0) * CORES + core]
    along_y = [chip_at(0, 1) * CORES + core, chip_at(0, -1) * CORES + core]
    first_axis = [along_z[way] * (1 - core) + along_y[way] * core for way in range(2)]
    second_axis = [along_y[way] * (1 - core) + along_z[way] * core for way in range(2)]
    axes = ((along_z, along_y), (along_y, along_z), (first_axis, second_axis))
    partner = (chip * CORES + (1 - core), tp)
    after = (lax.rem(sp + 1, sp_size), tp)
    before = (lax.rem(sp + sp_size - 1, sp_size), tp)
    tp_right = lax.rem(tp + 1, TP)
    tp_left = lax.rem(tp + TP - 1, TP)
    tp_far = lax.rem(tp + 2, TP)
    sides = [(sp, tp_right), (sp, tp_left)]
    far = (sp, tp_far)

    barrier = pltpu.get_barrier_semaphore()
    greeted = [(axis[way], tp) for axis in (along_z, along_y) for way in range(2)]
    greeted += [partner, after, before, far] + sides
    for device in greeted:
        pl.semaphore_signal(barrier, inc=1, device_id=device, device_id_type=MESH)

    own_rows = pl.ds(pl.multiple_of(core * depth, depth), depth)
    loads = [
        pltpu.make_async_copy(src, dst, local_sem.at[i])
        for i, (src, dst) in enumerate(
            (
                (q_hbm, q_all),
                (k_hbm, k_all.at[pl.ds(HALF, rows)]),
                (v_hbm, v_all.at[pl.ds(HALF, rows)]),
                (doc_hbm, doc_all.at[:, pl.ds(HALF, rows)]),
                (w_out_hbm, w_out),
                (res_hbm, res_all),
                (gain_one_hbm, gains_in.at[pl.ds(0, 1)]),
                (gain_two_hbm, gains_in.at[pl.ds(1, 1)]),
                (wg_hbm, gate_w.at[own_rows]),
                (wu_hbm, up_w.at[own_rows]),
                (wd_hbm, down_w.at[own_rows]),
            )
        )
    ]
    for load in loads:
        load.start()

    def remote(src, dst, send, recv, device):
        return pltpu.make_async_remote_copy(
            src_ref=src, dst_ref=dst, send_sem=send, recv_sem=recv, device_id=device, device_id_type=MESH
        )

    def launch(copy):
        copy.start()

    def arrive(copy):
        copy.wait_recv()

    def wait_bytes(ref, sem):
        remote(ref, ref, sem, sem, partner).wait_recv()

    low, high = (pl.ds(0, HALF), pl.ds(rows - HALF, HALF))
    into_low, into_high = (pl.ds(0, HALF), pl.ds(HALF + rows, HALF))

    def launch_halos():
        for i, (src, dst) in enumerate(((k_hbm, k_all), (v_hbm, v_all))):
            launch(remote(src.at[high], dst.at[into_low], halo_send.at[i], halo_recv.at[i], after))
            launch(remote(src.at[low], dst.at[into_high], halo_send.at[i], halo_recv.at[i], before))
        launch(
            remote(doc_hbm.at[:, high], doc_all.at[:, into_low], halo_send.at[2], halo_recv.at[2], after)
        )
        launch(
            remote(doc_hbm.at[:, low], doc_all.at[:, into_high], halo_send.at[2], halo_recv.at[2], before)
        )

    def halo_refs():
        edge = pl.ds(0, 2 * HALF)
        return (k_all.at[edge], v_all.at[edge], doc_all.at[:, edge])

    def halo_wait():
        for i, ref in enumerate(halo_refs()):
            wait_bytes(ref, halo_recv.at[i])

    sources = (wg_hbm, wu_hbm, wd_hbm)
    buffers = (gate_w, up_w, down_w)

    def slot_for(kind, offset, core_id):
        straight, swapped = SLOT[offset], SLOT[offset[::-1]]
        if kind == 0:
            return straight
        if kind == 1:
            return swapped
        return straight * (1 - core_id) + swapped * core_id

    def place(kind, offset, half, core_id):
        start = slot_for(kind, offset, core_id) * wide + core_id * depth
        if half is None:
            return buffers[kind].at[pl.ds(pl.multiple_of(start, depth), depth)]
        return buffers[kind].at[pl.ds(pl.multiple_of(start + half * sub_rows, sub_rows), sub_rows)]

    def ring(kind, number, way, outgoing):
        axis, src_offset, dst_offset, halved = message(number, way)
        half = way if halved else None
        dst = place(kind, dst_offset, half, core)
        if not outgoing:
            src = dst
        elif src_offset == (0, 0):
            src = sources[kind] if half is None else sources[kind].at[pl.ds(half * sub_rows, sub_rows)]
        else:
            src = place(kind, src_offset, half, core)
        to = (axes[kind][axis][way if outgoing else 1 - way], tp)
        return remote(src, dst, ring_send.at[kind], ring_recv.at[kind, way, number], to)

    def pair(kind, offset, half):
        dst = place(kind, offset, half, core)
        src = sources[kind] if offset == (0, 0) else dst
        slot = SLOT[offset]
        if kind == 2:
            sem = down_recv.at[chunk_of(slot)]
        else:
            sem = pair_recv.at[kind, segment_of(slot)]
        return remote(src, dst, pair_send.at[kind], sem, partner)

    def begin(kinds):
        for number in (1, 2):
            for kind in kinds:
                for way in range(2):
                    launch(ring(kind, number, way, True))

    def tick(number, kinds):
        for kind in kinds:
            for way in range(2):
                arrive(ring(kind, number, way, False))
        for follower in FOLLOW.get(number, ()):
            for kind in kinds:
                for way in range(2):
                    launch(ring(kind, follower, way, True))
        for kind in kinds:
            for way in range(2):
                _, _, offset, halved = message(number, way)
                launch(pair(kind, offset, way if halved else None))

    weights_tick = lambda number: tick(number, (0, 1))
    down_tick = lambda number: tick(number, (2,))

    def segment_wait(segment):
        lo, hi = SEGMENTS[segment]
        for kind in range(2):
            wait_bytes(buffers[kind].at[pl.ds(0, (hi - lo) * depth)], pair_recv.at[kind, segment])

    for load in loads[:4]:
        load.wait()
    span = rows + 2 * HALF
    at = lax.broadcasted_iota(jnp.int32, (1, span), 1) + (sp * rows - HALF)
    inside = jnp.logical_and(at >= 0, at < sp_size * rows)
    reach = 3 * HALF
    repeat = q_hbm.shape[1] // HEAD
    offset_of = lax.broadcasted_iota(jnp.int32, (HALF, reach), 1) - lax.broadcasted_iota(
        jnp.int32, (HALF, reach), 0
    )
    near = jnp.logical_and(offset_of >= 0, offset_of <= 2 * HALF)

    def attend(block):
        here = slice(block * HALF, (block + 1) * HALF)
        there = slice(block * HALF, block * HALF + reach)
        doc_row = doc_all[:, (block + 1) * HALF : (block + 2) * HALF]
        doc_query = jnp.broadcast_to(doc_row, (HALF, HALF)).T
        doc_keys = jnp.where(inside[:, there], doc_all[:, there], -1)
        same = jnp.concatenate([doc_query] * 3, 1) == doc_keys
        allowed = jnp.logical_and(near, same)
        key_blk = k_all[there, :]
        value_blk = v_all[there, :]
        for h in range(repeat):
            lanes = slice(h * HEAD, (h + 1) * HEAD)
            scores = lax.dot_general(
                q_all[here, lanes], key_blk, (((1,), (1,)), ((), ())), preferred_element_type=F32
            ) * HEAD ** (-0.5)
            scores = jnp.where(allowed, scores, NEGATIVE)
            sink = jnp.full((1, 1), sink_ref[h], F32)
            top = jnp.maximum(jnp.max(scores, -1, keepdims=True), sink)
            weights = jnp.exp(scores - top)
            total = jnp.sum(weights, -1, keepdims=True) + jnp.exp(sink - top)
            summed = jnp.dot(weights.astype(BF16), value_blk, preferred_element_type=F32)
            att[here, lanes] = (summed / total).astype(BF16)

    def token_rows_of(j):
        return pl.ds(pl.multiple_of(j * token_rows, token_rows), token_rows)

    def send_tokens():
        for j in (tp_far, tp_right, tp_left):
            launch(
                remote(att.at[token_rows_of(j)], tokens.at[tp], tok_send.at[0], tok_recv.at[0], (sp, j))
            )
        tokens[pl.ds(tp, 1)] = att[token_rows_of(tp), :][None]

    def order_gains():
        for slot in range(CHIPS):
            gains[:, slot_lanes(slot)] = gains_in[:, chip_lanes(slot)]

    def project():
        for first, second in zip(range(0, CHIPS, 2), range(1, CHIPS, 2)):
            picks = (chip_lanes(first), chip_lanes(second))
            mixed = ALPHA * jnp.concatenate([res_all[:, pick] for pick in picks], 1).astype(F32)
            for j in range(TP):
                deep = slice(j * 256, (j + 1) * 256)
                mixed += jnp.dot(
                    tokens[j],
                    jnp.concatenate([w_out[deep, pick] for pick in picks], 1),
                    preferred_element_type=F32,
                )
            pre[:, first * wide : (second + 1) * wide] = mixed

    strip = 32

    def norm_rows(first, last):
        @pl.loop(first // strip, last // strip)
        def _(t):
            here = pl.ds(pl.multiple_of(t * strip, strip), strip)
            normed[here, :] = layer_norm(pre[here, :], gains[0:1, :]).astype(BF16)

    def piece_rows(index):
        return pl.ds(index * half_rows, half_rows)

    ROUTES = ((0, 0, 2), (1, 1, 3), (0, 1, 4), (1, 0, 5), (0, 2, 6), (1, 3, 7))

    def norm_copy(route):
        way, src, dst = ROUTES[route]
        return remote(
            normed.at[piece_rows(src)],
            normed.at[piece_rows(dst)],
            norm_send.at[0],
            norm_recv.at[route],
            sides[way],
        )

    def norm_arrive(route):
        way, _, dst = ROUTES[route]
        slot = normed.at[piece_rows(dst)]
        arrive(remote(slot, slot, norm_send.at[0], norm_recv.at[route], sides[1 - way]))

    def gate_up(top, bottom, lo, hi, lanes):
        deep = slice(lo * wide, hi * wide)
        gate = jnp.dot(normed[top:bottom, deep], gate_w[deep, lanes], preferred_element_type=F32)
        up = jnp.dot(normed[top:bottom, deep], up_w[deep, lanes], preferred_element_type=F32)
        if lo > 0:
            gate += gate_acc[top:bottom, lanes]
            up += up_acc[top:bottom, lanes]
        if hi < CHIPS:
            gate_acc[top:bottom, lanes] = gate
            up_acc[top:bottom, lanes] = up
        else:
            hidden[top:bottom, lanes] = (gate / (1.0 + jnp.exp(-gate)) * up).astype(BF16)

    def gate_up_tiles(top, bottom, lo, hi, first, last):
        @pl.loop(first, last)
        def _(t):
            gate_up(top, bottom, lo, hi, pl.ds(pl.multiple_of(t * 256, 256), 256))

    def gate_up_rest(top, bottom, lo, hi):
        gate_up(top, bottom, lo, hi, slice(units // 256 * 256, units))

    def gate_up_range(top, bottom, lo, hi):
        gate_up_tiles(top, bottom, lo, hi, 0, units // 256)
        gate_up_rest(top, bottom, lo, hi)

    def dest(index):
        return pl.ds(index * token_rows, token_rows)

    OWN, LEFT, RIGHT, FAR = range(4)
    ORDER = (0, 1, 2, 4, 5, 3, 6, 7)

    def down_chunk(k):
        a, b = CHUNKS[k]
        if b == a + 1:
            weights = down_w[a * wide : (b + 1) * wide, :]
        else:
            weights = jnp.concatenate([down_w[s * wide : (s + 1) * wide, :] for s in (a, b)], 0)
        part = lax.dot_general(
            hidden[...], weights, (((1,), (1,)), ((), ())), preferred_element_type=F32
        ).astype(BF16)
        for to, source in enumerate(ORDER):
            for slot, lanes in ((a, slice(0, wide)), (b, slice(wide, 2 * wide))):
                parts[slot, to * half_rows : (to + 1) * half_rows, :] = part[
                    source * half_rows : (source + 1) * half_rows, lanes
                ]
        launch(remote(parts.at[a, dest(FAR)], relays.at[0, k], sum_send.at[0], relay_recv.at[0, k], sides[0]))
        launch(remote(parts.at[b, dest(FAR)], relays.at[1, k], sum_send.at[0], relay_recv.at[1, k], sides[1]))
        launch(remote(parts.at[b, dest(RIGHT)], arrived.at[k, 1], sum_send.at[0], sum_recv.at[k], sides[0]))
        launch(remote(parts.at[a, dest(LEFT)], arrived.at[k, 2], sum_send.at[0], sum_recv.at[k], sides[1]))

    def relay_chunk(k):
        for way, slot, to, index in ((0, CHUNKS[k][0], RIGHT, 0), (1, CHUNKS[k][1], LEFT, 3)):
            held = relays.at[way, k]
            arrive(remote(held, held, sum_send.at[0], relay_recv.at[way, k], sides[1 - way]))
            here = dest(to)
            parts[slot, here, :] = (
                parts[slot, here, :].astype(F32) + relays[way, k].astype(F32)
            ).astype(BF16)
            launch(
                remote(parts.at[slot, here], arrived.at[k, index], sum_send.at[0], sum_recv.at[k], sides[way])
            )

    def finish_chunk(k):
        wait_bytes(arrived.at[k], sum_recv.at[k])
        for slot, left, right in ((CHUNKS[k][0], 0, 2), (CHUNKS[k][1], 1, 3)):
            down = (
                parts[slot, dest(OWN), :].astype(F32)
                + arrived[k, left].astype(F32)
                + arrived[k, right].astype(F32)
            )
            pre[:, slot_lanes(slot)] = ALPHA * normed[0:token_rows, slot_lanes(slot)].astype(F32) + down

    def final_norm():
        @pl.loop(0, token_rows // strip)
        def _(t):
            here = pl.ds(pl.multiple_of(t * strip, strip), strip)
            result = layer_norm(pre[here, :], gains[1:2, :]).astype(BF16)
            for slot in range(CHIPS):
                out_ref[here, chip_lanes(slot)] = result[:, slot_lanes(slot)]

    def sends_wait():
        def gone(ref, sem):
            remote(ref, ref, sem, sem, partner).wait_send()

        for i, ref in enumerate(halo_refs()):
            gone(ref, halo_send.at[i])
        for kind in range(3):
            gone(buffers[kind].at[pl.ds(0, (CHIPS - 1) * depth)], ring_send.at[kind])
            gone(buffers[kind].at[pl.ds(0, CHIPS * depth)], pair_send.at[kind])
        gone(tokens.at[pl.ds(0, TP - 1)], tok_send.at[0])
        gone(normed.at[pl.ds(0, 6 * half_rows)], norm_send.at[0])
        gone(parts.at[pl.ds(0, 12)], sum_send.at[0])

    attend(1)
    attend(2)
    pl.semaphore_wait(barrier, len(greeted))
    launch_halos()
    begin((0, 1))
    for kind in range(3):
        launch(pair(kind, (0, 0), None))
    halo_wait()
    attend(0)
    attend(3)
    send_tokens()
    weights_tick(1)
    for load in loads[4:]:
        load.wait()
    order_gains()
    wait_bytes(tokens.at[pl.ds(0, TP - 1)], tok_recv.at[0])
    project()
    norm_rows(0, half_rows)
    launch(norm_copy(0))
    norm_rows(half_rows, token_rows)
    for route in (1, 2, 3):
        launch(norm_copy(route))
    weights_tick(2)
    weights_tick(3)
    weights_tick(4)
    for route in (0, 1):
        norm_arrive(route)
    for route in (4, 5):
        launch(norm_copy(route))
    weights_tick(5)
    segment_wait(0)
    gate_up_range(0, 256, 0, 5)
    weights_tick(6)
    segment_wait(1)
    gate_up_range(0, 256, 5, 11)
    weights_tick(7)
    begin((2,))
    for route in (2, 3):
        norm_arrive(route)
    gate_up_range(256, 384, 0, 11)
    weights_tick(8)
    weights_tick(9)
    for route in (4, 5):
        norm_arrive(route)
    gate_up_range(384, 512, 0, 11)
    weights_tick(10)
    segment_wait(2)
    gate_up_tiles(0, 512, 11, 16, 0, 3)
    down_tick(1)
    gate_up_tiles(0, 512, 11, 16, 3, 5)
    gate_up_rest(0, 512, 11, 16)
    down_tick(2)
    needs = (2, 2, 4, 5, 6, 9, 9, 10)
    done = 2
    for k in range(len(CHUNKS)):
        while done < needs[k]:
            done += 1
            down_tick(done)
        wait_bytes(down_w.at[pl.ds(0, wide)], down_recv.at[k])
        down_chunk(k)
        if k >= 1:
            relay_chunk(k - 1)
        if k >= 3:
            finish_chunk(k - 3)
    relay_chunk(7)
    for k in (5, 6, 7):
        finish_chunk(k)
    final_norm()
    sends_wait()


def solution(mesh):
    def per_device(
        queries,
        keys,
        values,
        doc_ids,
        sink_logit,
        residual_in,
        w_out,
        gain_one,
        w_gate,
        w_up,
        w_down,
        gain_two,
    ):
        rows = queries.shape[0]
        token_rows, width = residual_in.shape
        units = w_gate.shape[1]
        span = rows + 2 * HALF
        dma = pltpu.SemaphoreType.DMA
        vmem, anywhere = (pl.BlockSpec(memory_space=pltpu.VMEM), pl.BlockSpec(memory_space=pl.ANY))
        return pl.pallas_call(
            kernel,
            out_shape=jax.ShapeDtypeStruct((token_rows, width), BF16),
            in_specs=[pl.BlockSpec(memory_space=pltpu.SMEM)] + [anywhere] * 11,
            out_specs=vmem,
            scratch_shapes=[
                pltpu.VMEM(queries.shape, BF16),
                pltpu.VMEM((span, keys.shape[1]), BF16),
                pltpu.VMEM((span, keys.shape[1]), BF16),
                pltpu.VMEM((1, span), jnp.int32),
                pltpu.VMEM((2, width), F32),
                pltpu.VMEM((2, width), F32),
                pltpu.VMEM((token_rows, width), BF16),
                pltpu.VMEM(w_out.shape, BF16),
                pltpu.VMEM((width, units), BF16),
                pltpu.VMEM((width, units), BF16),
                pltpu.VMEM((width, units), BF16),
                pltpu.VMEM(queries.shape, BF16),
                pltpu.VMEM((TP, token_rows, queries.shape[1]), BF16),
                pltpu.VMEM((token_rows, width), F32),
                pltpu.VMEM((rows, width), BF16),
                pltpu.VMEM((rows, units), F32),
                pltpu.VMEM((rows, units), F32),
                pltpu.VMEM((rows, units), BF16),
                pltpu.VMEM((CHIPS, rows, width // CHIPS), BF16),
                pltpu.VMEM((2, len(CHUNKS), token_rows, width // CHIPS), BF16),
                pltpu.VMEM((len(CHUNKS), 4, token_rows, width // CHIPS), BF16),
                dma((11,)),
                dma((3,)),
                dma((3,)),
                dma((3,)),
                dma((3, 2, LAST + 1)),
                dma((3,)),
                dma((2, len(SEGMENTS))),
                dma((len(CHUNKS),)),
                dma((1,)),
                dma((1,)),
                dma((1,)),
                dma((6,)),
                dma((1,)),
                dma((2, len(CHUNKS))),
                dma((len(CHUNKS),)),
            ],
            compiler_params=pltpu.CompilerParams(
                collective_id=0, has_side_effects=True, vmem_limit_bytes=62 * 2**20
            ),
        )(
            sink_logit,
            queries,
            residual_in,
            gain_one[None, :],
            gain_two[None, :],
            keys,
            values,
            doc_ids[None, :],
            w_out,
            w_gate,
            w_up,
            w_down.T,
        )

    in_specs = (
        P("sp", "tp"),
        P("sp", "tp"),
        P("sp", "tp"),
        P("sp"),
        P("tp"),
        P(("sp", "tp"), None),
        P(),
        P(),
        P("sp", "tp"),
        P("sp", "tp"),
        P("tp", "sp"),
        P(),
    )
    return jax.shard_map(
        per_device, mesh=mesh, in_specs=in_specs, out_specs=P(("sp", "tp"), None), check_vma=False
    )
```

time: 99.8 us -> 79.4 us (0.80); the launches traced: 99.6 us -> 78.2 us
  Pallas kernels: 97.8 us -> 76.3 us
    pallas_call x1, Pallas kernels: 97.8 us -> 76.3 us  [per_device(): pl.pallas_call(kernel, out_shape=jax.ShapeDtypeStruct((token_rows, width)...]
where the time goes in v2:
time: 79.4 us; the launch traced here: 78.2 us
  Pallas kernels  76.3 us (96%)
  local copies, waits for them, and re-layouts  1.88 us (2%)
    pallas_call x1, Pallas kernels, per_device(): pl.pallas_call(kernel, out_shape=jax.ShapeDtypeStruct((token_rows, width)...  76.3 us
    unnamed x1, local copies, waits for them, and re-layouts  1.88 us

profile of v2, /device:TPU:1, one launch (start us, length us, event | category | flops | bytes accessed | tf_op | source)
XLA Modules:
  0.0 78.2 jit_solution(1601025020731078805)
XLA Ops:
  0.0 76.3 %shard_map.118 = bf16[128,2048]{1,0:T(8,128)(2,1)} custom-call(f32[2]{0:T(128)} %sink_ref.1, bf16[512,256]{1,0:T(8,128)(2,1)} %q_hbm.1, bf16[128,2048]{1,0:T(8,128)(2,1)} %res_hbm.1, f32[1,2048]{1,0:T(1,128)} %bitcast.5, f32[1,2048]{1,0:T(1,128)} %bitcast.6, bf16[512,128]{1,0:T(8,128)(2,1)} %k_hbm.1, bf16[512,128]{1,0:T(8,128)(2,1)} %v_hbm.1, ...), custom_call_target="tpu_custom_call" | custom-call | tf_op jit(solution)/shard_map/pallas_call | solution.py:578
  76.3 1.9 %copy.14 = bf16[128,2048]{1,0:T(8,128)(2,1)} copy(bf16[128,2048]{1,0:T(8,128)(2,1)} %shard_map.118) | data formatting | bytes 1048576

commit v3 on v2

--- a/solution.py
+++ b/solution.py
@@ -36,7 +36,7 @@
     (2, 2),
 )
 SLOT = {offset: slot for slot, offset in enumerate(OFFSETS)}
-SEGMENTS = ((0, 5), (5, 11), (11, 16))
+SEGMENTS = ((0, 5), (5, 11), (11, 15), (15, 16))
 CHUNKS = ((1, 2), (3, 4), (5, 6), (7, 8), (9, 10), (11, 12), (13, 14), (0, 15))
 LAST = 10
 
@@ -211,19 +211,17 @@
     def wait_bytes(ref, sem):
         remote(ref, ref, sem, sem, partner).wait_recv()
 
-    low, high = (pl.ds(0, HALF), pl.ds(rows - HALF, HALF))
+    low, high = (pl.ds(HALF, HALF), pl.ds(rows, HALF))
     into_low, into_high = (pl.ds(0, HALF), pl.ds(HALF + rows, HALF))
 
     def launch_halos():
-        for i, (src, dst) in enumerate(((k_hbm, k_all), (v_hbm, v_all))):
-            launch(remote(src.at[high], dst.at[into_low], halo_send.at[i], halo_recv.at[i], after))
-            launch(remote(src.at[low], dst.at[into_high], halo_send.at[i], halo_recv.at[i], before))
-        launch(
-            remote(doc_hbm.at[:, high], doc_all.at[:, into_low], halo_send.at[2], halo_recv.at[2], after)
-        )
-        launch(
-            remote(doc_hbm.at[:, low], doc_all.at[:, into_high], halo_send.at[2], halo_recv.at[2], before)
-        )
+        for i, ref in enumerate((k_all, v_all)):
+            launch(remote(ref.at[high], ref.at[into_low], halo_send.at[i], halo_recv.at[i], after))
+            launch(remote(ref.at[low], ref.at[into_high], halo_send.at[i], halo_recv.at[i], before))
+        for src, dst, to in ((high, into_low, after), (low, into_high, before)):
+            launch(
+                remote(doc_all.at[:, src], doc_all.at[:, dst], halo_send.at[2], halo_recv.at[2], to)
+            )
 
     def halo_refs():
         edge = pl.ds(0, 2 * HALF)
@@ -233,7 +231,6 @@
         for i, ref in enumerate(halo_refs()):
             wait_bytes(ref, halo_recv.at[i])
 
-    sources = (wg_hbm, wu_hbm, wd_hbm)
     buffers = (gate_w, up_w, down_w)
 
     def slot_for(kind, offset, core_id):
@@ -254,24 +251,18 @@
         axis, src_offset, dst_offset, halved = message(number, way)
         half = way if halved else None
         dst = place(kind, dst_offset, half, core)
-        if not outgoing:
-            src = dst
-        elif src_offset == (0, 0):
-            src = sources[kind] if half is None else sources[kind].at[pl.ds(half * sub_rows, sub_rows)]
-        else:
-            src = place(kind, src_offset, half, core)
+        src = place(kind, src_offset, half, core) if outgoing else dst
         to = (axes[kind][axis][way if outgoing else 1 - way], tp)
         return remote(src, dst, ring_send.at[kind], ring_recv.at[kind, way, number], to)
 
     def pair(kind, offset, half):
         dst = place(kind, offset, half, core)
-        src = sources[kind] if offset == (0, 0) else dst
         slot = SLOT[offset]
         if kind == 2:
             sem = down_recv.at[chunk_of(slot)]
         else:
             sem = pair_recv.at[kind, segment_of(slot)]
-        return remote(src, dst, pair_send.at[kind], sem, partner)
+        return remote(dst, dst, pair_send.at[kind], sem, partner)
 
     def begin(kinds):
         for number in (1, 2):
@@ -300,8 +291,6 @@
         for kind in range(2):
             wait_bytes(buffers[kind].at[pl.ds(0, (hi - lo) * depth)], pair_recv.at[kind, segment])
 
-    for load in loads[:4]:
-        load.wait()
     span = rows + 2 * HALF
     at = lax.broadcasted_iota(jnp.int32, (1, span), 1) + (sp * rows - HALF)
     inside = jnp.logical_and(at >= 0, at < sp_size * rows)
@@ -422,6 +411,7 @@
     ORDER = (0, 1, 2, 4, 5, 3, 6, 7)
 
     def down_chunk(k):
+        wait_bytes(down_w.at[pl.ds(0, wide)], down_recv.at[k])
         a, b = CHUNKS[k]
         if b == a + 1:
             weights = down_w[a * wide : (b + 1) * wide, :]
@@ -437,6 +427,9 @@
                 ]
         launch(remote(parts.at[a, dest(FAR)], relays.at[0, k], sum_send.at[0], relay_recv.at[0, k], sides[0]))
         launch(remote(parts.at[b, dest(FAR)], relays.at[1, k], sum_send.at[0], relay_recv.at[1, k], sides[1]))
+
+    def plain_chunk(k):
+        a, b = CHUNKS[k]
         launch(remote(parts.at[b, dest(RIGHT)], arrived.at[k, 1], sum_send.at[0], sum_recv.at[k], sides[0]))
         launch(remote(parts.at[a, dest(LEFT)], arrived.at[k, 2], sum_send.at[0], sum_recv.at[k], sides[1]))
 
@@ -483,19 +476,23 @@
         gone(normed.at[pl.ds(0, 6 * half_rows)], norm_send.at[0])
         gone(parts.at[pl.ds(0, 12)], sum_send.at[0])
 
-    attend(1)
-    attend(2)
     pl.semaphore_wait(barrier, len(greeted))
+    for load in loads[:4]:
+        load.wait()
     launch_halos()
+    for load in loads[8:]:
+        load.wait()
     begin((0, 1))
     for kind in range(3):
         launch(pair(kind, (0, 0), None))
+    attend(1)
+    attend(2)
     halo_wait()
     attend(0)
     attend(3)
     send_tokens()
     weights_tick(1)
-    for load in loads[4:]:
+    for load in loads[4:8]:
         load.wait()
     order_gains()
     wait_bytes(tokens.at[pl.ds(0, TP - 1)], tok_recv.at[0])
@@ -528,28 +525,57 @@
     for route in (4, 5):
         norm_arrive(route)
     gate_up_range(384, 512, 0, 11)
+    segment_wait(2)
+    gate_up_tiles(0, 512, 11, 15, 0, 2)
     weights_tick(10)
-    segment_wait(2)
-    gate_up_tiles(0, 512, 11, 16, 0, 3)
+    gate_up_tiles(0, 512, 11, 15, 2, 5)
+    gate_up_rest(0, 512, 11, 15)
+    segment_wait(3)
+    gate_up_tiles(0, 512, 15, 16, 0, 2)
     down_tick(1)
-    gate_up_tiles(0, 512, 11, 16, 3, 5)
-    gate_up_rest(0, 512, 11, 16)
+    gate_up_tiles(0, 512, 15, 16, 2, 5)
+    gate_up_rest(0, 512, 15, 16)
     down_tick(2)
-    needs = (2, 2, 4, 5, 6, 9, 9, 10)
-    done = 2
-    for k in range(len(CHUNKS)):
-        while done < needs[k]:
-            done += 1
-            down_tick(done)
-        wait_bytes(down_w.at[pl.ds(0, wide)], down_recv.at[k])
-        down_chunk(k)
-        if k >= 1:
-            relay_chunk(k - 1)
-        if k >= 3:
-            finish_chunk(k - 3)
+    down_chunk(0)
+    plain_chunk(0)
+    down_tick(3)
+    down_chunk(1)
+    plain_chunk(1)
+    down_tick(4)
+    down_chunk(2)
+    plain_chunk(2)
+    down_tick(5)
+    relay_chunk(0)
+    down_chunk(3)
+    plain_chunk(3)
+    down_tick(6)
+    relay_chunk(1)
+    down_tick(7)
+    down_chunk(4)
+    plain_chunk(4)
+    relay_chunk(2)
+    down_tick(8)
+    down_tick(9)
+    down_chunk(5)
+    plain_chunk(5)
+    relay_chunk(3)
+    down_chunk(6)
+    relay_chunk(4)
+    down_tick(10)
+    down_chunk(7)
+    plain_chunk(6)
+    relay_chunk(5)
+    plain_chunk(7)
+    finish_chunk(0)
+    finish_chunk(1)
+    finish_chunk(2)
+    relay_chunk(6)
     relay_chunk(7)
-    for k in (5, 6, 7):
-        finish_chunk(k)
+    finish_chunk(3)
+    finish_chunk(4)
+    finish_chunk(5)
+    finish_chunk(6)
+    finish_chunk(7)
     final_norm()
     sends_wait()
 
@@ -577,7 +603,7 @@
         vmem, anywhere = (pl.BlockSpec(memory_space=pltpu.VMEM), pl.BlockSpec(memory_space=pl.ANY))
         return pl.pallas_call(
             kernel,
-            out_shape=jax.ShapeDtypeStruct((token_rows, width), BF16),
+            out_shape=pltpu.VMEM((token_rows, width), BF16),
             in_specs=[pl.BlockSpec(memory_space=pltpu.SMEM)] + [anywhere] * 11,
             out_specs=vmem,
             scratch_shapes=[

time: 79.4 us -> 73 us (0.919); the launches traced: 78.2 us -> 72.9 us
  Pallas kernels: 76.3 us -> 72.1 us
  local copies, waits for them, and re-layouts: 1.88 us -> 0.8 us
    pallas_call x1, Pallas kernels: 76.3 us -> 72.1 us  [per_device(): pl.pallas_call(kernel, out_shape=pltpu.VMEM((token_rows, width), BF16), i...]
    unnamed x1, local copies, waits for them, and re-layouts: 1.88 us -> 0.8 us
where the time goes in v3:
time: 73 us; the launch traced here: 72.9 us
  Pallas kernels  72.1 us (99%)
  local copies, waits for them, and re-layouts  0.8 us (1%)
    pallas_call x1, Pallas kernels, per_device(): pl.pallas_call(kernel, out_shape=pltpu.VMEM((token_rows, width), BF16), i...  72.1 us

profile of v3, /device:TPU:1, one launch (start us, length us, event | category | flops | bytes accessed | tf_op | source)
XLA Modules:
  0.0 72.9 jit_solution(11343878156838904087)
XLA Ops:
  0.0 72.1 %shard_map.118 = bf16[128,2048]{1,0:T(8,128)(2,1)S(1)} custom-call(f32[2]{0:T(128)} %sink_ref.1, bf16[512,256]{1,0:T(8,128)(2,1)} %q_hbm.1, bf16[128,2048]{1,0:T(8,128)(2,1)} %res_hbm.1, f32[1,2048]{1,0:T(1,128)} %bitcast.5, f32[1,2048]{1,0:T(1,128)} %bitcast.6, bf16[512,128]{1,0:T(8,128)(2,1)} %k_hbm.1, bf16[512,128]{1,0:T(8,128)(2,1)} %v_hbm.1, ...), custom_call_target="tpu_custom_call" | custom-call | tf_op jit(solution)/shard_map/pallas_call | solution.py:604
  72.1 0.8 %copy.14 = bf16[128,2048]{1,0:T(8,128)(2,1)} copy(bf16[128,2048]{1,0:T(8,128)(2,1)S(1)} %shard_map.118) | data formatting | bytes 1048576

commit v4 on v3

--- a/solution.py
+++ b/solution.py
@@ -36,8 +36,8 @@
     (2, 2),
 )
 SLOT = {offset: slot for slot, offset in enumerate(OFFSETS)}
-SEGMENTS = ((0, 5), (5, 11), (11, 15), (15, 16))
-CHUNKS = ((1, 2), (3, 4), (5, 6), (7, 8), (9, 10), (11, 12), (13, 14), (0, 15))
+SEGMENTS = ((0, 4), (4, 10), (10, 16))
+CHUNKS = ((1, 3), (2, 4), (5, 6), (7, 8), (9, 10), (11, 13), (12, 14), (0, 15))
 LAST = 10
 
 
@@ -233,51 +233,46 @@
 
     buffers = (gate_w, up_w, down_w)
 
-    def slot_for(kind, offset, core_id):
+    def slot_for(kind, offset):
         straight, swapped = SLOT[offset], SLOT[offset[::-1]]
-        if kind == 0:
-            return straight
-        if kind == 1:
-            return swapped
-        return straight * (1 - core_id) + swapped * core_id
+        return swapped if kind == 1 else straight
 
     def place(kind, offset, half, core_id):
-        start = slot_for(kind, offset, core_id) * wide + core_id * depth
+        start = slot_for(kind, offset) * wide + core_id * depth
         if half is None:
             return buffers[kind].at[pl.ds(pl.multiple_of(start, depth), depth)]
         return buffers[kind].at[pl.ds(pl.multiple_of(start + half * sub_rows, sub_rows), sub_rows)]
 
-    def ring(kind, number, way, outgoing):
+    def ring(kind, number, way):
         axis, src_offset, dst_offset, halved = message(number, way)
         half = way if halved else None
         dst = place(kind, dst_offset, half, core)
-        src = place(kind, src_offset, half, core) if outgoing else dst
-        to = (axes[kind][axis][way if outgoing else 1 - way], tp)
-        return remote(src, dst, ring_send.at[kind], ring_recv.at[kind, way, number], to)
+        src = place(kind, src_offset, half, core)
+        to = (axes[kind][axis][way], tp)
+        return remote(src, dst, ring_send.at[kind], ring_recv.at[kind // 2, number - 1], to)
 
     def pair(kind, offset, half):
         dst = place(kind, offset, half, core)
-        slot = SLOT[offset]
+        slot = slot_for(kind, offset)
         if kind == 2:
             sem = down_recv.at[chunk_of(slot)]
         else:
-            sem = pair_recv.at[kind, segment_of(slot)]
+            sem = pair_recv.at[segment_of(slot)]
         return remote(dst, dst, pair_send.at[kind], sem, partner)
 
-    def begin(kinds):
-        for number in (1, 2):
-            for kind in kinds:
-                for way in range(2):
-                    launch(ring(kind, number, way, True))
-
-    def tick(number, kinds):
+    def begin(number, kinds):
         for kind in kinds:
             for way in range(2):
-                arrive(ring(kind, number, way, False))
+                launch(ring(kind, number, way))
+
+    def tick(number, kinds):
+        halved = message(number, 0)[3]
+        total = 2 * len(kinds) * (sub_rows if halved else depth)
+        wait_bytes(buffers[kinds[0]].at[pl.ds(0, total)], ring_recv.at[kinds[0] // 2, number - 1])
         for follower in FOLLOW.get(number, ()):
             for kind in kinds:
                 for way in range(2):
-                    launch(ring(kind, follower, way, True))
+                    launch(ring(kind, follower, way))
         for kind in kinds:
             for way in range(2):
                 _, _, offset, halved = message(number, way)
@@ -288,8 +283,7 @@
 
     def segment_wait(segment):
         lo, hi = SEGMENTS[segment]
-        for kind in range(2):
-            wait_bytes(buffers[kind].at[pl.ds(0, (hi - lo) * depth)], pair_recv.at[kind, segment])
+        wait_bytes(gate_w.at[pl.ds(0, 2 * (hi - lo) * depth)], pair_recv.at[segment])
 
     span = rows + 2 * HALF
     at = lax.broadcasted_iota(jnp.int32, (1, span), 1) + (sp * rows - HALF)
@@ -328,30 +322,37 @@
         return pl.ds(pl.multiple_of(j * token_rows, token_rows), token_rows)
 
     def send_tokens():
-        for j in (tp_far, tp_right, tp_left):
+        for j, into in ((tp_far, 3), (tp_right, 1), (tp_left, 2)):
             launch(
-                remote(att.at[token_rows_of(j)], tokens.at[tp], tok_send.at[0], tok_recv.at[0], (sp, j))
+                remote(
+                    att.at[token_rows_of(j)], tokens.at[into], tok_send.at[0], tok_recv.at[into // 3], (sp, j)
+                )
             )
-        tokens[pl.ds(tp, 1)] = att[token_rows_of(tp), :][None]
+        tokens[0] = att[token_rows_of(tp), :]
 
     def order_gains():
         for slot in range(CHIPS):
             gains[:, slot_lanes(slot)] = gains_in[:, chip_lanes(slot)]
 
-    def project():
+    def project(held):
         for first, second in zip(range(0, CHIPS, 2), range(1, CHIPS, 2)):
             picks = (chip_lanes(first), chip_lanes(second))
-            mixed = ALPHA * jnp.concatenate([res_all[:, pick] for pick in picks], 1).astype(F32)
-            for j in range(TP):
-                deep = slice(j * 256, (j + 1) * 256)
+            lanes = slice(first * wide, (second + 1) * wide)
+            if held[0] == 0:
+                mixed = ALPHA * jnp.concatenate([res_all[:, pick] for pick in picks], 1).astype(F32)
+            else:
+                mixed = pre[:, lanes]
+            for j in held:
+                cols = q_hbm.shape[1]
+                deep = pl.ds(pl.multiple_of((tp, tp_left, tp_right, tp_far)[j] * cols, cols), cols)
                 mixed += jnp.dot(
                     tokens[j],
                     jnp.concatenate([w_out[deep, pick] for pick in picks], 1),
                     preferred_element_type=F32,
                 )
-            pre[:, first * wide : (second + 1) * wide] = mixed
-
-    strip = 32
+            pre[:, lanes] = mixed
+
+    strip = 64
 
     def norm_rows(first, last):
         @pl.loop(first // strip, last // strip)
@@ -370,14 +371,12 @@
             normed.at[piece_rows(src)],
             normed.at[piece_rows(dst)],
             norm_send.at[0],
-            norm_recv.at[route],
+            norm_recv.at[route // 2],
             sides[way],
         )
 
-    def norm_arrive(route):
-        way, _, dst = ROUTES[route]
-        slot = normed.at[piece_rows(dst)]
-        arrive(remote(slot, slot, norm_send.at[0], norm_recv.at[route], sides[1 - way]))
+    def norm_arrive(stage):
+        wait_bytes(normed.at[pl.ds(0, 2 * half_rows)], norm_recv.at[stage])
 
     def gate_up(top, bottom, lo, hi, lanes):
         deep = slice(lo * wide, hi * wide)
@@ -425,8 +424,8 @@
                 parts[slot, to * half_rows : (to + 1) * half_rows, :] = part[
                     source * half_rows : (source + 1) * half_rows, lanes
                 ]
-        launch(remote(parts.at[a, dest(FAR)], relays.at[0, k], sum_send.at[0], relay_recv.at[0, k], sides[0]))
-        launch(remote(parts.at[b, dest(FAR)], relays.at[1, k], sum_send.at[0], relay_recv.at[1, k], sides[1]))
+        launch(remote(parts.at[a, dest(FAR)], relays.at[k, 0], sum_send.at[0], relay_recv.at[k], sides[0]))
+        launch(remote(parts.at[b, dest(FAR)], relays.at[k, 1], sum_send.at[0], relay_recv.at[k], sides[1]))
 
     def plain_chunk(k):
         a, b = CHUNKS[k]
@@ -434,16 +433,20 @@
         launch(remote(parts.at[a, dest(LEFT)], arrived.at[k, 2], sum_send.at[0], sum_recv.at[k], sides[1]))
 
     def relay_chunk(k):
+        wait_bytes(relays.at[k], relay_recv.at[k])
         for way, slot, to, index in ((0, CHUNKS[k][0], RIGHT, 0), (1, CHUNKS[k][1], LEFT, 3)):
-            held = relays.at[way, k]
-            arrive(remote(held, held, sum_send.at[0], relay_recv.at[way, k], sides[1 - way]))
             here = dest(to)
             parts[slot, here, :] = (
-                parts[slot, here, :].astype(F32) + relays[way, k].astype(F32)
+                parts[slot, here, :].astype(F32) + relays[k, way].astype(F32)
             ).astype(BF16)
             launch(
                 remote(parts.at[slot, here], arrived.at[k, index], sum_send.at[0], sum_recv.at[k], sides[way])
             )
+
+    first_core = lax.broadcasted_iota(jnp.int32, (token_rows, wide), 1) < depth
+
+    def prepare_sum():
+        pre[...] = ALPHA * normed[0:token_rows, :].astype(F32)
 
     def finish_chunk(k):
         wait_bytes(arrived.at[k], sum_recv.at[k])
@@ -453,7 +456,12 @@
                 + arrived[k, left].astype(F32)
                 + arrived[k, right].astype(F32)
             )
-            pre[:, slot_lanes(slot)] = ALPHA * normed[0:token_rows, slot_lanes(slot)].astype(F32) + down
+            swapped = SLOT[OFFSETS[slot][::-1]]
+            if swapped == slot:
+                pre[:, slot_lanes(slot)] += down
+            else:
+                pre[:, slot_lanes(slot)] += jnp.where(first_core, down, 0.0)
+                pre[:, slot_lanes(swapped)] += jnp.where(first_core, 0.0, down)
 
     def final_norm():
         @pl.loop(0, token_rows // strip)
@@ -482,7 +490,8 @@
     launch_halos()
     for load in loads[8:]:
         load.wait()
-    begin((0, 1))
+    begin(1, (0, 1))
+    begin(2, (0, 1))
     for kind in range(3):
         launch(pair(kind, (0, 0), None))
     attend(1)
@@ -495,8 +504,10 @@
     for load in loads[4:8]:
         load.wait()
     order_gains()
-    wait_bytes(tokens.at[pl.ds(0, TP - 1)], tok_recv.at[0])
-    project()
+    wait_bytes(tokens.at[pl.ds(0, 2)], tok_recv.at[0])
+    project((0, 1, 2))
+    wait_bytes(tokens.at[3], tok_recv.at[1])
+    project((3,))
     norm_rows(0, half_rows)
     launch(norm_copy(0))
     norm_rows(half_rows, token_rows)
@@ -504,65 +515,62 @@
         launch(norm_copy(route))
     weights_tick(2)
     weights_tick(3)
+    prepare_sum()
     weights_tick(4)
-    for route in (0, 1):
-        norm_arrive(route)
+    norm_arrive(0)
     for route in (4, 5):
         launch(norm_copy(route))
     weights_tick(5)
     segment_wait(0)
-    gate_up_range(0, 256, 0, 5)
+    gate_up_range(0, 256, 0, 4)
     weights_tick(6)
     segment_wait(1)
-    gate_up_range(0, 256, 5, 11)
+    gate_up_range(0, 256, 4, 10)
     weights_tick(7)
-    begin((2,))
-    for route in (2, 3):
-        norm_arrive(route)
-    gate_up_range(256, 384, 0, 11)
+    begin(1, (2,))
+    norm_arrive(1)
+    gate_up_range(256, 384, 0, 10)
     weights_tick(8)
     weights_tick(9)
-    for route in (4, 5):
-        norm_arrive(route)
-    gate_up_range(384, 512, 0, 11)
+    norm_arrive(2)
+    begin(2, (2,))
+    gate_up_tiles(384, 512, 0, 10, 0, 3)
+    weights_tick(10)
+    gate_up_tiles(384, 512, 0, 10, 3, 5)
+    gate_up_rest(384, 512, 0, 10)
     segment_wait(2)
-    gate_up_tiles(0, 512, 11, 15, 0, 2)
-    weights_tick(10)
-    gate_up_tiles(0, 512, 11, 15, 2, 5)
-    gate_up_rest(0, 512, 11, 15)
-    segment_wait(3)
-    gate_up_tiles(0, 512, 15, 16, 0, 2)
+    gate_up_tiles(0, 512, 10, 16, 0, 2)
     down_tick(1)
-    gate_up_tiles(0, 512, 15, 16, 2, 5)
-    gate_up_rest(0, 512, 15, 16)
+    gate_up_tiles(0, 512, 10, 16, 2, 5)
+    gate_up_rest(0, 512, 10, 16)
     down_tick(2)
     down_chunk(0)
     plain_chunk(0)
-    down_tick(3)
     down_chunk(1)
     plain_chunk(1)
+    down_tick(3)
     down_tick(4)
+    relay_chunk(0)
     down_chunk(2)
     plain_chunk(2)
     down_tick(5)
-    relay_chunk(0)
+    down_tick(6)
+    relay_chunk(1)
     down_chunk(3)
     plain_chunk(3)
-    down_tick(6)
-    relay_chunk(1)
     down_tick(7)
     down_chunk(4)
     plain_chunk(4)
+    down_tick(8)
     relay_chunk(2)
-    down_tick(8)
     down_tick(9)
     down_chunk(5)
     plain_chunk(5)
+    down_tick(10)
+    down_chunk(6)
     relay_chunk(3)
-    down_chunk(6)
+    down_chunk(7)
     relay_chunk(4)
-    down_tick(10)
-    down_chunk(7)
     plain_chunk(6)
     relay_chunk(5)
     plain_chunk(7)
@@ -626,22 +634,22 @@
                 pltpu.VMEM((rows, units), F32),
                 pltpu.VMEM((rows, units), BF16),
                 pltpu.VMEM((CHIPS, rows, width // CHIPS), BF16),
-                pltpu.VMEM((2, len(CHUNKS), token_rows, width // CHIPS), BF16),
+                pltpu.VMEM((len(CHUNKS), 2, token_rows, width // CHIPS), BF16),
                 pltpu.VMEM((len(CHUNKS), 4, token_rows, width // CHIPS), BF16),
                 dma((11,)),
                 dma((3,)),
                 dma((3,)),
                 dma((3,)),
-                dma((3, 2, LAST + 1)),
+                dma((2, LAST)),
                 dma((3,)),
-                dma((2, len(SEGMENTS))),
+                dma((len(SEGMENTS),)),
                 dma((len(CHUNKS),)),
                 dma((1,)),
+                dma((2,)),
                 dma((1,)),
+                dma((3,)),
                 dma((1,)),
-                dma((6,)),
-                dma((1,)),
-                dma((2, len(CHUNKS))),
+                dma((len(CHUNKS),)),
                 dma((len(CHUNKS),)),
             ],
             compiler_params=pltpu.CompilerParams(

time: 73 us -> 70.4 us (0.964)
  Pallas kernels: 72.1 us -> 69.5 us
    pallas_call x1, Pallas kernels: 72.1 us -> 69.5 us  [per_device(): pl.pallas_call(kernel, out_shape=pltpu.VMEM((token_rows, width), BF16), i...]
where the time goes in v4:
time: 70.4 us; the launch traced here: 70.3 us
  Pallas kernels  69.5 us (99%)
  local copies, waits for them, and re-layouts  0.8 us (1%)
    pallas_call x1, Pallas kernels, per_device(): pl.pallas_call(kernel, out_shape=pltpu.VMEM((token_rows, width), BF16), i...  69.5 us

profile of v4, /device:TPU:1, one launch (start us, length us, event | category | flops | bytes accessed | tf_op | source)
XLA Modules:
  0.0 70.3 jit_solution(5681311964492609439)
XLA Ops:
  0.0 69.5 %shard_map.118 = bf16[128,2048]{1,0:T(8,128)(2,1)S(1)} custom-call(f32[2]{0:T(128)} %sink_ref.1, bf16[512,256]{1,0:T(8,128)(2,1)} %q_hbm.1, bf16[128,2048]{1,0:T(8,128)(2,1)} %res_hbm.1, f32[1,2048]{1,0:T(1,128)} %bitcast.5, f32[1,2048]{1,0:T(1,128)} %bitcast.6, bf16[512,128]{1,0:T(8,128)(2,1)} %k_hbm.1, bf16[512,128]{1,0:T(8,128)(2,1)} %v_hbm.1, ...), custom_call_target="tpu_custom_call" | custom-call | tf_op jit(solution)/shard_map/pallas_call | solution.py:612
  69.5 0.8 %copy.14 = bf16[128,2048]{1,0:T(8,128)(2,1)} copy(bf16[128,2048]{1,0:T(8,128)(2,1)S(1)} %shard_map.118) | data formatting | bytes 1048576

commit v5 on v4

--- a/solution.py
+++ b/solution.py
@@ -36,8 +36,8 @@
     (2, 2),
 )
 SLOT = {offset: slot for slot, offset in enumerate(OFFSETS)}
-SEGMENTS = ((0, 4), (4, 10), (10, 16))
-CHUNKS = ((1, 3), (2, 4), (5, 6), (7, 8), (9, 10), (11, 13), (12, 14), (0, 15))
+SEGMENTS = ((0, 4), (4, 10), (10, 14), (14, 16))
+CHUNKS = ((1, 3), (2, 4), (0, 9), (5, 6), (7, 8), (11, 13), (12, 14), (10, 15))
 LAST = 10
 
 
@@ -59,6 +59,7 @@
 
 
 FOLLOW = {1: (3, 4, 5), 2: (6,), 3: (7,), 4: (8,), 5: (9,), 7: (10,)}
+DOWN_FOLLOW = {1: (3, 4, 5), 3: (7, 6), 4: (8,), 5: (9,), 7: (10,)}
 
 
 def segment_of(slot):
@@ -194,7 +195,7 @@
             )
         )
     ]
-    for load in loads:
+    for load in loads[:4] + loads[8:]:
         load.start()
 
     def remote(src, dst, send, recv, device):
@@ -269,7 +270,7 @@
         halved = message(number, 0)[3]
         total = 2 * len(kinds) * (sub_rows if halved else depth)
         wait_bytes(buffers[kinds[0]].at[pl.ds(0, total)], ring_recv.at[kinds[0] // 2, number - 1])
-        for follower in FOLLOW.get(number, ()):
+        for follower in (DOWN_FOLLOW if kinds[0] == 2 else FOLLOW).get(number, ()):
             for kind in kinds:
                 for way in range(2):
                     launch(ring(kind, follower, way))
@@ -391,57 +392,54 @@
         else:
             hidden[top:bottom, lanes] = (gate / (1.0 + jnp.exp(-gate)) * up).astype(BF16)
 
-    def gate_up_tiles(top, bottom, lo, hi, first, last):
-        @pl.loop(first, last)
-        def _(t):
-            gate_up(top, bottom, lo, hi, pl.ds(pl.multiple_of(t * 256, 256), 256))
-
-    def gate_up_rest(top, bottom, lo, hi):
-        gate_up(top, bottom, lo, hi, slice(units // 256 * 256, units))
-
     def gate_up_range(top, bottom, lo, hi):
-        gate_up_tiles(top, bottom, lo, hi, 0, units // 256)
-        gate_up_rest(top, bottom, lo, hi)
-
-    def dest(index):
-        return pl.ds(index * token_rows, token_rows)
-
-    OWN, LEFT, RIGHT, FAR = range(4)
-    ORDER = (0, 1, 2, 4, 5, 3, 6, 7)
-
-    def down_chunk(k):
-        wait_bytes(down_w.at[pl.ds(0, wide)], down_recv.at[k])
+        for start in range(0, units, 256):
+            gate_up(top, bottom, lo, hi, slice(start, min(start + 256, units)))
+
+    LEFT, RIGHT, OWN, FAR = range(4)
+    def down_rows(k, top, bottom, pieces):
         a, b = CHUNKS[k]
         if b == a + 1:
             weights = down_w[a * wide : (b + 1) * wide, :]
         else:
             weights = jnp.concatenate([down_w[s * wide : (s + 1) * wide, :] for s in (a, b)], 0)
         part = lax.dot_general(
-            hidden[...], weights, (((1,), (1,)), ((), ())), preferred_element_type=F32
+            hidden[top:bottom, :], weights, (((1,), (1,)), ((), ())), preferred_element_type=F32
         ).astype(BF16)
-        for to, source in enumerate(ORDER):
-            for slot, lanes in ((a, slice(0, wide)), (b, slice(wide, 2 * wide))):
-                parts[slot, to * half_rows : (to + 1) * half_rows, :] = part[
+        for source, to in enumerate(pieces):
+            for side, lanes in ((0, slice(0, wide)), (1, slice(wide, 2 * wide))):
+                parts[to // 2, k, side, to % 2 * half_rows : (to % 2 + 1) * half_rows, :] = part[
                     source * half_rows : (source + 1) * half_rows, lanes
                 ]
-        launch(remote(parts.at[a, dest(FAR)], relays.at[k, 0], sum_send.at[0], relay_recv.at[k], sides[0]))
-        launch(remote(parts.at[b, dest(FAR)], relays.at[k, 1], sum_send.at[0], relay_recv.at[k], sides[1]))
+
+    def down_far(k):
+        wait_bytes(down_w.at[pl.ds(0, wide)], down_recv.at[k])
+        down_rows(k, 3 * token_rows, 4 * token_rows, (6, 7))
+        for way in range(2):
+            launch(
+                remote(
+                    parts.at[FAR, k, way], relays.at[k, way], sum_send.at[0], relay_recv.at[k], sides[way]
+                )
+            )
+
+    def down_rest(k):
+        down_rows(k, 0, 3 * token_rows, (4, 5, 0, 3, 1, 2))
 
     def plain_chunk(k):
-        a, b = CHUNKS[k]
-        launch(remote(parts.at[b, dest(RIGHT)], arrived.at[k, 1], sum_send.at[0], sum_recv.at[k], sides[0]))
-        launch(remote(parts.at[a, dest(LEFT)], arrived.at[k, 2], sum_send.at[0], sum_recv.at[k], sides[1]))
-
-    def relay_chunk(k):
+        for way, to, side in ((0, RIGHT, 1), (1, LEFT, 0)):
+            launch(
+                remote(
+                    parts.at[to, k, side], arrived.at[k, to, side], sum_send.at[0], sum_recv.at[k], sides[way]
+                )
+            )
+
+    def relay_chunk(k, whole):
         wait_bytes(relays.at[k], relay_recv.at[k])
-        for way, slot, to, index in ((0, CHUNKS[k][0], RIGHT, 0), (1, CHUNKS[k][1], LEFT, 3)):
-            here = dest(to)
-            parts[slot, here, :] = (
-                parts[slot, here, :].astype(F32) + relays[k, way].astype(F32)
-            ).astype(BF16)
-            launch(
-                remote(parts.at[slot, here], arrived.at[k, index], sum_send.at[0], sum_recv.at[k], sides[way])
-            )
+        for way, to in ((0, RIGHT), (1, LEFT)):
+            parts[to, k, way] = (parts[to, k, way].astype(F32) + relays[k, way].astype(F32)).astype(BF16)
+            piece = (to, k) if whole else (to, k, way)
+            into = (k, to) if whole else (k, to, way)
+            launch(remote(parts.at[piece], arrived.at[into], sum_send.at[0], sum_recv.at[k], sides[way]))
 
     first_core = lax.broadcasted_iota(jnp.int32, (token_rows, wide), 1) < depth
 
@@ -450,11 +448,11 @@
 
     def finish_chunk(k):
         wait_bytes(arrived.at[k], sum_recv.at[k])
-        for slot, left, right in ((CHUNKS[k][0], 0, 2), (CHUNKS[k][1], 1, 3)):
+        for side, slot in enumerate(CHUNKS[k]):
             down = (
-                parts[slot, dest(OWN), :].astype(F32)
-                + arrived[k, left].astype(F32)
-                + arrived[k, right].astype(F32)
+                parts[OWN, k, side].astype(F32)
+                + arrived[k, LEFT, side].astype(F32)
+                + arrived[k, RIGHT, side].astype(F32)
             )
             swapped = SLOT[OFFSETS[slot][::-1]]
             if swapped == slot:
@@ -482,11 +480,12 @@
             gone(buffers[kind].at[pl.ds(0, CHIPS * depth)], pair_send.at[kind])
         gone(tokens.at[pl.ds(0, TP - 1)], tok_send.at[0])
         gone(normed.at[pl.ds(0, 6 * half_rows)], norm_send.at[0])
-        gone(parts.at[pl.ds(0, 12)], sum_send.at[0])
-
-    pl.semaphore_wait(barrier, len(greeted))
+        gone(parts.at[pl.ds(0, 3)], sum_send.at[0])
+
     for load in loads[:4]:
         load.wait()
+    attend(1)
+    pl.semaphore_wait(barrier, len(greeted))
     launch_halos()
     for load in loads[8:]:
         load.wait()
@@ -494,7 +493,8 @@
     begin(2, (0, 1))
     for kind in range(3):
         launch(pair(kind, (0, 0), None))
-    attend(1)
+    for load in loads[4:8]:
+        load.start()
     attend(2)
     halo_wait()
     attend(0)
@@ -534,51 +534,58 @@
     weights_tick(9)
     norm_arrive(2)
     begin(2, (2,))
-    gate_up_tiles(384, 512, 0, 10, 0, 3)
+    gate_up_range(384, 512, 0, 10)
     weights_tick(10)
-    gate_up_tiles(384, 512, 0, 10, 3, 5)
-    gate_up_rest(384, 512, 0, 10)
     segment_wait(2)
-    gate_up_tiles(0, 512, 10, 16, 0, 2)
+    gate_up_range(0, 512, 10, 14)
     down_tick(1)
-    gate_up_tiles(0, 512, 10, 16, 2, 5)
-    gate_up_rest(0, 512, 10, 16)
+    segment_wait(3)
+    gate_up_range(0, 256, 14, 16)
     down_tick(2)
-    down_chunk(0)
+    gate_up_range(256, 512, 14, 16)
+    down_far(0)
+    down_far(1)
+    down_rest(0)
     plain_chunk(0)
-    down_chunk(1)
+    down_tick(3)
+    down_rest(1)
     plain_chunk(1)
-    down_tick(3)
     down_tick(4)
-    relay_chunk(0)
-    down_chunk(2)
+    relay_chunk(0, False)
+    down_far(2)
+    relay_chunk(1, False)
+    down_rest(2)
     plain_chunk(2)
     down_tick(5)
-    down_tick(6)
-    relay_chunk(1)
-    down_chunk(3)
+    down_far(3)
+    down_rest(3)
     plain_chunk(3)
     down_tick(7)
-    down_chunk(4)
+    down_far(4)
+    relay_chunk(2, False)
+    down_tick(6)
+    down_rest(4)
     plain_chunk(4)
     down_tick(8)
-    relay_chunk(2)
+    down_far(5)
+    relay_chunk(3, False)
     down_tick(9)
-    down_chunk(5)
+    down_rest(5)
     plain_chunk(5)
     down_tick(10)
-    down_chunk(6)
-    relay_chunk(3)
-    down_chunk(7)
-    relay_chunk(4)
+    down_far(6)
+    relay_chunk(4, False)
+    down_far(7)
+    down_rest(6)
     plain_chunk(6)
-    relay_chunk(5)
+    relay_chunk(5, False)
+    down_rest(7)
     plain_chunk(7)
+    relay_chunk(6, False)
     finish_chunk(0)
     finish_chunk(1)
     finish_chunk(2)
-    relay_chunk(6)
-    relay_chunk(7)
+    relay_chunk(7, False)
     finish_chunk(3)
     finish_chunk(4)
     finish_chunk(5)
@@ -633,9 +640,9 @@
                 pltpu.VMEM((rows, units), F32),
                 pltpu.VMEM((rows, units), F32),
                 pltpu.VMEM((rows, units), BF16),
-                pltpu.VMEM((CHIPS, rows, width // CHIPS), BF16),
+                pltpu.VMEM((4, len(CHUNKS), 2, token_rows, width // CHIPS), BF16),
                 pltpu.VMEM((len(CHUNKS), 2, token_rows, width // CHIPS), BF16),
-                pltpu.VMEM((len(CHUNKS), 4, token_rows, width // CHIPS), BF16),
+                pltpu.VMEM((len(CHUNKS), 2, 2, token_rows, width // CHIPS), BF16),
                 dma((11,)),
                 dma((3,)),
                 dma((3,)),

time: 70.4 us -> 67.9 us (0.964)
  Pallas kernels: 69.5 us -> 66.9 us
    pallas_call x1, Pallas kernels: 69.5 us -> 66.9 us  [per_device(): pl.pallas_call(kernel, out_shape=pltpu.VMEM((token_rows, width), BF16), i...]
where the time goes in v5:
time: 67.9 us; the launch traced here: 67.7 us
  Pallas kernels  66.9 us (99%)
  local copies, waits for them, and re-layouts  0.8 us (1%)
    pallas_call x1, Pallas kernels, per_device(): pl.pallas_call(kernel, out_shape=pltpu.VMEM((token_rows, width), BF16), i...  66.9 us

profile of v5, /device:TPU:1, one launch (start us, length us, event | category | flops | bytes accessed | tf_op | source)
XLA Modules:
  0.0 67.7 jit_solution(3196693419314566940)
XLA Ops:
  0.0 66.9 %shard_map.118 = bf16[128,2048]{1,0:T(8,128)(2,1)S(1)} custom-call(f32[2]{0:T(128)} %sink_ref.1, bf16[512,256]{1,0:T(8,128)(2,1)} %q_hbm.1, bf16[128,2048]{1,0:T(8,128)(2,1)} %res_hbm.1, f32[1,2048]{1,0:T(1,128)} %bitcast.5, f32[1,2048]{1,0:T(1,128)} %bitcast.6, bf16[512,128]{1,0:T(8,128)(2,1)} %k_hbm.1, bf16[512,128]{1,0:T(8,128)(2,1)} %v_hbm.1, ...), custom_call_target="tpu_custom_call" | custom-call | tf_op jit(solution)/shard_map/pallas_call | solution.py:619
  66.9 0.8 %copy.14 = bf16[128,2048]{1,0:T(8,128)(2,1)} copy(bf16[128,2048]{1,0:T(8,128)(2,1)S(1)} %shard_map.118) | data formatting | bytes 1048576

commit v6 on v5

--- a/solution.py
+++ b/solution.py
@@ -99,9 +99,7 @@
     gains,
     res_all,
     w_out,
-    gate_w,
-    up_w,
-    down_w,
+    weights,
     att,
     tokens,
     pre,
@@ -128,6 +126,7 @@
     relay_recv,
     sum_recv,
 ):
+    gate_w, up_w, down_w = (weights.at[i] for i in range(3))
     sp = lax.axis_index("sp")
     tp = lax.axis_index("tp")
     sp_size = CHIPS * CORES
@@ -177,26 +176,18 @@
         pl.semaphore_signal(barrier, inc=1, device_id=device, device_id_type=MESH)
 
     own_rows = pl.ds(pl.multiple_of(core * depth, depth), depth)
-    loads = [
-        pltpu.make_async_copy(src, dst, local_sem.at[i])
-        for i, (src, dst) in enumerate(
-            (
-                (q_hbm, q_all),
-                (k_hbm, k_all.at[pl.ds(HALF, rows)]),
-                (v_hbm, v_all.at[pl.ds(HALF, rows)]),
-                (doc_hbm, doc_all.at[:, pl.ds(HALF, rows)]),
-                (w_out_hbm, w_out),
-                (res_hbm, res_all),
-                (gain_one_hbm, gains_in.at[pl.ds(0, 1)]),
-                (gain_two_hbm, gains_in.at[pl.ds(1, 1)]),
-                (wg_hbm, gate_w.at[own_rows]),
-                (wu_hbm, up_w.at[own_rows]),
-                (wd_hbm, down_w.at[own_rows]),
-            )
-        )
-    ]
-    for load in loads[:4] + loads[8:]:
-        load.start()
+    def load(src, dst, sem):
+        pltpu.make_async_copy(src, dst, local_sem.at[sem]).start()
+
+    def loaded(ref, sem):
+        pltpu.make_async_copy(ref, ref, local_sem.at[sem]).wait()
+
+    load(k_hbm, k_all.at[pl.ds(HALF, rows)], 0)
+    load(v_hbm, v_all.at[pl.ds(HALF, rows)], 0)
+    load(q_hbm, q_all, 0)
+    load(doc_hbm, doc_all.at[:, pl.ds(HALF, rows)], 1)
+    for i, src in enumerate((wg_hbm, wu_hbm, wd_hbm)):
+        load(src, weights.at[i, own_rows], 2)
 
     def remote(src, dst, send, recv, device):
         return pltpu.make_async_remote_copy(
@@ -217,16 +208,15 @@
 
     def launch_halos():
         for i, ref in enumerate((k_all, v_all)):
-            launch(remote(ref.at[high], ref.at[into_low], halo_send.at[i], halo_recv.at[i], after))
-            launch(remote(ref.at[low], ref.at[into_high], halo_send.at[i], halo_recv.at[i], before))
+            launch(remote(ref.at[high], ref.at[into_low], halo_send.at[0], halo_recv.at[0], after))
+            launch(remote(ref.at[low], ref.at[into_high], halo_send.at[0], halo_recv.at[0], before))
         for src, dst, to in ((high, into_low, after), (low, into_high, before)):
             launch(
-                remote(doc_all.at[:, src], doc_all.at[:, dst], halo_send.at[2], halo_recv.at[2], to)
+                remote(doc_all.at[:, src], doc_all.at[:, dst], halo_send.at[1], halo_recv.at[1], to)
             )
 
     def halo_refs():
-        edge = pl.ds(0, 2 * HALF)
-        return (k_all.at[edge], v_all.at[edge], doc_all.at[:, edge])
+        return (k_all.at[pl.ds(0, 4 * HALF)], doc_all.at[:, pl.ds(0, 2 * HALF)])
 
     def halo_wait():
         for i, ref in enumerate(halo_refs()):
@@ -250,7 +240,7 @@
         dst = place(kind, dst_offset, half, core)
         src = place(kind, src_offset, half, core)
         to = (axes[kind][axis][way], tp)
-        return remote(src, dst, ring_send.at[kind], ring_recv.at[kind // 2, number - 1], to)
+        return remote(src, dst, ring_send.at[0], ring_recv.at[kind // 2, number - 1], to)
 
     def pair(kind, offset, half):
         dst = place(kind, offset, half, core)
@@ -259,7 +249,7 @@
             sem = down_recv.at[chunk_of(slot)]
         else:
             sem = pair_recv.at[segment_of(slot)]
-        return remote(dst, dst, pair_send.at[kind], sem, partner)
+        return remote(dst, dst, pair_send.at[0], sem, partner)
 
     def begin(number, kinds):
         for kind in kinds:
@@ -462,9 +452,8 @@
                 pre[:, slot_lanes(swapped)] += jnp.where(first_core, 0.0, down)
 
     def final_norm():
-        @pl.loop(0, token_rows // strip)
-        def _(t):
-            here = pl.ds(pl.multiple_of(t * strip, strip), strip)
+        for t in range(token_rows // strip):
+            here = pl.ds(t * strip, strip)
             result = layer_norm(pre[here, :], gains[1:2, :]).astype(BF16)
             for slot in range(CHIPS):
                 out_ref[here, chip_lanes(slot)] = result[:, slot_lanes(slot)]
@@ -475,34 +464,35 @@
 
         for i, ref in enumerate(halo_refs()):
             gone(ref, halo_send.at[i])
-        for kind in range(3):
-            gone(buffers[kind].at[pl.ds(0, (CHIPS - 1) * depth)], ring_send.at[kind])
-            gone(buffers[kind].at[pl.ds(0, CHIPS * depth)], pair_send.at[kind])
+        gone(weights.at[:, pl.ds(0, (CHIPS - 1) * depth)], ring_send.at[0])
+        gone(weights.at[:, pl.ds(0, CHIPS * depth)], pair_send.at[0])
         gone(tokens.at[pl.ds(0, TP - 1)], tok_send.at[0])
         gone(normed.at[pl.ds(0, 6 * half_rows)], norm_send.at[0])
         gone(parts.at[pl.ds(0, 3)], sum_send.at[0])
 
-    for load in loads[:4]:
-        load.wait()
+    loaded(normed.at[pl.ds(0, rows // 4)], 0)
+    loaded(doc_all.at[:, pl.ds(HALF, rows)], 1)
     attend(1)
     pl.semaphore_wait(barrier, len(greeted))
     launch_halos()
-    for load in loads[8:]:
-        load.wait()
+    loaded(gate_w.at[pl.ds(0, 3 * depth)], 2)
     begin(1, (0, 1))
     begin(2, (0, 1))
     for kind in range(3):
         launch(pair(kind, (0, 0), None))
-    for load in loads[4:8]:
-        load.start()
+    load(w_out_hbm, w_out, 3)
+    load(res_hbm, res_all, 4)
+    for i, src in enumerate((gain_one_hbm, gain_two_hbm)):
+        load(src, gains_in.at[pl.ds(i, 1)], 5)
     attend(2)
     halo_wait()
     attend(0)
     attend(3)
     send_tokens()
     weights_tick(1)
-    for load in loads[4:8]:
-        load.wait()
+    loaded(w_out, 3)
+    loaded(res_all, 4)
+    loaded(gains_in, 5)
     order_gains()
     wait_bytes(tokens.at[pl.ds(0, 2)], tok_recv.at[0])
     project((0, 1, 2))
@@ -535,9 +525,10 @@
     norm_arrive(2)
     begin(2, (2,))
     gate_up_range(384, 512, 0, 10)
+    segment_wait(2)
+    gate_up_range(0, 128, 10, 14)
     weights_tick(10)
-    segment_wait(2)
-    gate_up_range(0, 512, 10, 14)
+    gate_up_range(128, 512, 10, 14)
     down_tick(1)
     segment_wait(3)
     gate_up_range(0, 256, 14, 16)
@@ -630,9 +621,7 @@
                 pltpu.VMEM((2, width), F32),
                 pltpu.VMEM((token_rows, width), BF16),
                 pltpu.VMEM(w_out.shape, BF16),
-                pltpu.VMEM((width, units), BF16),
-                pltpu.VMEM((width, units), BF16),
-                pltpu.VMEM((width, units), BF16),
+                pltpu.VMEM((3, width, units), BF16),
                 pltpu.VMEM(queries.shape, BF16),
                 pltpu.VMEM((TP, token_rows, queries.shape[1]), BF16),
                 pltpu.VMEM((token_rows, width), F32),
@@ -643,12 +632,12 @@
                 pltpu.VMEM((4, len(CHUNKS), 2, token_rows, width // CHIPS), BF16),
                 pltpu.VMEM((len(CHUNKS), 2, token_rows, width // CHIPS), BF16),
                 pltpu.VMEM((len(CHUNKS), 2, 2, token_rows, width // CHIPS), BF16),
-                dma((11,)),
-                dma((3,)),
-                dma((3,)),
-                dma((3,)),
+                dma((6,)),
+                dma((2,)),
+                dma((2,)),
+                dma((1,)),
                 dma((2, LAST)),
-                dma((3,)),
+                dma((1,)),
                 dma((len(SEGMENTS),)),
                 dma((len(CHUNKS),)),
                 dma((1,)),

time: 67.9 us -> 67.4 us (level)
  no operation moved by 1% of the time
where the time goes in v6:
time: 67.4 us; the launch traced here: 67.3 us
  Pallas kernels  66.5 us (99%)
  local copies, waits for them, and re-layouts  0.8 us (1%)
    pallas_call x1, Pallas kernels, per_device(): pl.pallas_call(kernel, out_shape=pltpu.VMEM((token_rows, width), BF16), i...  66.5 us

profile of v6, /device:TPU:1, one launch (start us, length us, event | category | flops | bytes accessed | tf_op | source)
XLA Modules:
  0.0 67.3 jit_solution(7845310006370312121)
XLA Ops:
  0.0 66.5 %shard_map.118 = bf16[128,2048]{1,0:T(8,128)(2,1)S(1)} custom-call(f32[2]{0:T(128)} %sink_ref.1, bf16[512,256]{1,0:T(8,128)(2,1)} %q_hbm.1, bf16[128,2048]{1,0:T(8,128)(2,1)} %res_hbm.1, f32[1,2048]{1,0:T(1,128)} %bitcast.5, f32[1,2048]{1,0:T(1,128)} %bitcast.6, bf16[512,128]{1,0:T(8,128)(2,1)} %k_hbm.1, bf16[512,128]{1,0:T(8,128)(2,1)} %v_hbm.1, ...), custom_call_target="tpu_custom_call" | custom-call | tf_op jit(solution)/shard_map/pallas_call | solution.py:610
  66.5 0.8 %copy.14 = bf16[128,2048]{1,0:T(8,128)(2,1)} copy(bf16[128,2048]{1,0:T(8,128)(2,1)S(1)} %shard_map.118) | data formatting | bytes 1048576

commit v7 on v6

--- a/solution.py
+++ b/solution.py
@@ -531,18 +531,17 @@
     gate_up_range(128, 512, 10, 14)
     down_tick(1)
     segment_wait(3)
-    gate_up_range(0, 256, 14, 16)
+    gate_up_range(0, 512, 14, 16)
+    down_far(0)
     down_tick(2)
-    gate_up_range(256, 512, 14, 16)
-    down_far(0)
-    down_far(1)
     down_rest(0)
     plain_chunk(0)
-    down_tick(3)
+    down_far(1)
     down_rest(1)
     plain_chunk(1)
+    down_tick(3)
+    relay_chunk(0, False)
     down_tick(4)
-    relay_chunk(0, False)
     down_far(2)
     relay_chunk(1, False)
     down_rest(2)

time: 67.4 us -> 67.4 us (level)
  no operation moved by 1% of the time
where the time goes in v7:
time: 67.4 us; the launch traced here: 67.2 us
  Pallas kernels  66.4 us (99%)
  local copies, waits for them, and re-layouts  0.8 us (1%)
    pallas_call x1, Pallas kernels, per_device(): pl.pallas_call(kernel, out_shape=pltpu.VMEM((token_rows, width), BF16), i...  66.4 us

profile of v7, /device:TPU:1, one launch (start us, length us, event | category | flops | bytes accessed | tf_op | source)
XLA Modules:
  0.0 67.2 jit_solution(14942270109205881780)
XLA Ops:
  0.0 66.4 %shard_map.118 = bf16[128,2048]{1,0:T(8,128)(2,1)S(1)} custom-call(f32[2]{0:T(128)} %sink_ref.1, bf16[512,256]{1,0:T(8,128)(2,1)} %q_hbm.1, bf16[128,2048]{1,0:T(8,128)(2,1)} %res_hbm.1, f32[1,2048]{1,0:T(1,128)} %bitcast.5, f32[1,2048]{1,0:T(1,128)} %bitcast.6, bf16[512,128]{1,0:T(8,128)(2,1)} %k_hbm.1, bf16[512,128]{1,0:T(8,128)(2,1)} %v_hbm.1, ...), custom_call_target="tpu_custom_call" | custom-call | tf_op jit(solution)/shard_map/pallas_call | solution.py:609
  66.4 0.8 %copy.14 = bf16[128,2048]{1,0:T(8,128)(2,1)} copy(bf16[128,2048]{1,0:T(8,128)(2,1)S(1)} %shard_map.118) | data formatting | bytes 1048576

commit v8 on v7

--- a/solution.py
+++ b/solution.py
@@ -540,13 +540,13 @@
     down_rest(1)
     plain_chunk(1)
     down_tick(3)
+    down_tick(4)
     relay_chunk(0, False)
-    down_tick(4)
     down_far(2)
+    down_tick(5)
     relay_chunk(1, False)
     down_rest(2)
     plain_chunk(2)
-    down_tick(5)
     down_far(3)
     down_rest(3)
     plain_chunk(3)

time: 67.4 us -> 67.5 us (level)
  no operation moved by 1% of the time
where the time goes in v8:
time: 67.5 us; the launch traced here: 67.3 us
  Pallas kernels  66.5 us (99%)
  local copies, waits for them, and re-layouts  0.8 us (1%)
    pallas_call x1, Pallas kernels, per_device(): pl.pallas_call(kernel, out_shape=pltpu.VMEM((token_rows, width), BF16), i...  66.5 us

profile of v8, /device:TPU:1, one launch (start us, length us, event | category | flops | bytes accessed | tf_op | source)
XLA Modules:
  0.0 67.3 jit_solution(10541872306359133616)
XLA Ops:
  0.0 66.5 %shard_map.118 = bf16[128,2048]{1,0:T(8,128)(2,1)S(1)} custom-call(f32[2]{0:T(128)} %sink_ref.1, bf16[512,256]{1,0:T(8,128)(2,1)} %q_hbm.1, bf16[128,2048]{1,0:T(8,128)(2,1)} %res_hbm.1, f32[1,2048]{1,0:T(1,128)} %bitcast.5, f32[1,2048]{1,0:T(1,128)} %bitcast.6, bf16[512,128]{1,0:T(8,128)(2,1)} %k_hbm.1, bf16[512,128]{1,0:T(8,128)(2,1)} %v_hbm.1, ...), custom_call_target="tpu_custom_call" | custom-call | tf_op jit(solution)/shard_map/pallas_call | solution.py:609
  66.5 0.8 %copy.14 = bf16[128,2048]{1,0:T(8,128)(2,1)} copy(bf16[128,2048]{1,0:T(8,128)(2,1)S(1)} %shard_map.118) | data formatting | bytes 1048576
